TPU v7x, 32 devices: a whole 2x2x4 slice. The times are simulated.
32 devices in a mesh: sp: 4 (over z), fs: 4 (over y, x), tp: 2 (over core).
Axes of the slice: x: 2, y: 2, z: 4, core: 2. Of those that a mesh axis runs over, the one named last changes fastest.
Arguments:
- tokens: bfloat16 [4, 1024, 2048], P('fs', 'sp'), may hold values from -6 to 6
- norm_gain: float32 [2048], replicated, may hold values from 0.1 to 1.9
- query_weight: bfloat16 [2048, 1024], P(('sp', 'fs'), 'tp'), may hold values from -0.125 to 0.125
- key_weight: bfloat16 [2048, 1024], P(('sp', 'fs'), 'tp'), may hold values from -0.125 to 0.125
- value_weight: bfloat16 [2048, 1024], P(('sp', 'fs'), 'tp'), may hold values from -0.125 to 0.125
- outgate_weight: bfloat16 [2048, 1024], P(('sp', 'fs'), 'tp'), may hold values from -0.125 to 0.125
- gate_weight: bfloat16 [4, 8, 2048], P(None, 'tp'), may hold values from -0.125 to 0.125
- gate_bias: float32 [4, 8], P(None, 'tp'), may hold values from -1 to 100
- decay_extra: float32 [4, 2, 8, 1024], P('fs', None, 'tp', 'sp'), may hold values from -0.75 to 0
- init_memory: float32 [4, 2, 8, 128, 128], P('fs', None, 'tp'), may hold values from -48 to 48
- init_normalizer: float32 [4, 2, 8, 128], P('fs', None, 'tp'), may hold values from -48 to 48
- head_gain: float32 [8, 128], P('tp'), may hold values from 0.1 to 1.9
- pool_weight: bfloat16 [2048, 2048], P(('sp', 'fs'), 'tp'), may hold values from -0.125 to 0.125
- mem_out_weight: bfloat16 [2048, 1024], P(('sp', 'fs'), 'tp'), may hold values from -0.1875 to 0.1875
- pool_out_weight: bfloat16 [2048, 2048], P(('sp', 'fs'), 'tp'), may hold values from -0.125 to 0.125
Outputs:
- mixed: bfloat16 [4, 1024, 2048], P('fs', ('sp', 'tp'))
All inputs are finite; a program needn't handle non-finite values.
Results may differ from a plain program's by a relative error of at most 0.014.
Values may be sent and summed in bfloat16 or wider, within the bound.
A program may use at most 64 MiB of HBM per device.

v0:
```python
import math

import jax
import jax.numpy as jnp
from jax import lax
from jax.sharding import PartitionSpec as P

HALO = 8


norm_eps = 1e-06
exact_mode = lax.Precision.HIGHEST


def carried_in(x, axis, combine, identity, reverse):
    length, position = (lax.axis_size(axis), lax.axis_index(axis))
    everything = jax.tree.map(lambda part: lax.all_gather(part, axis), x)
    start = jax.tree.map(
        lambda part, zero: jnp.broadcast_to(jnp.asarray(zero, part.dtype), part.shape), x, identity
    )

    def lap(k, before):
        at = length - 1 - k if reverse else k
        reached = at > position if reverse else at < position
        new = combine(before, jax.tree.map(lambda part: part[at], everything))
        return jax.tree.map(lambda a, b: jnp.where(reached, a, b), new, before)

    return lax.fori_loop(0, length, lap, start)


def padded_2(block, sides, width):
    for axis, dim in sides:
        count = lax.axis_size(axis)
        forward = [(i, i + 1) for i in range(count - 1)]
        backward = [(target, source) for source, target in forward]
        low = lax.ppermute(
            lax.slice_in_dim(block, block.shape[dim] - width, None, axis=dim), axis, forward
        )
        high = lax.ppermute(lax.slice_in_dim(block, 0, width, axis=dim), axis, backward)
        block = jnp.concatenate([low, block, high], axis=dim)
    return block


def block_output(
    query_rows, key_rows, value_rows, input_gate, log_forget, memory, normalizer, stabilizer
):
    block_len = query_rows.shape[1]
    key_scale = key_rows.shape[-1] ** (-0.5)
    lower_mask = jnp.tril(jnp.ones((block_len, block_len), dtype=bool))
    summed = jnp.cumsum(log_forget, axis=-1)
    log_decay = jnp.where(
        lower_mask, summed[:, :, None] - summed[:, None, :] + input_gate[:, None, :], -jnp.inf
    )
    log_carry = stabilizer[:, None] + summed
    running_max = jnp.maximum(log_carry, jnp.max(log_decay, axis=-1))
    scores = (
        jnp.einsum("btd,bsd->bts", query_rows, key_rows, preferred_element_type=jnp.float32)
        * key_scale
    )
    inner_weight = jnp.exp(log_decay - running_max[:, :, None]) * scores
    weight_rounded = inner_weight.astype(jnp.bfloat16)
    carry_weight = jnp.exp(log_carry - running_max)
    query_wide = query_rows.astype(jnp.float32)
    numerator = carry_weight[:, :, None] * jnp.einsum(
        "bed,btd->bte", memory, query_wide, precision=exact_mode
    )
    numerator = numerator + jnp.einsum(
        "bts,bse->bte", weight_rounded, value_rows, preferred_element_type=jnp.float32
    )
    denominator = carry_weight * jnp.einsum(
        "bd,btd->bt", normalizer, query_wide, precision=exact_mode
    )
    denominator = denominator + jnp.sum(inner_weight, axis=-1)
    return numerator / jnp.maximum(jnp.abs(denominator), jnp.exp(-running_max))[:, :, None]


def block_summary(key_rows, value_rows, input_gate, log_forget):
    key_wide = key_rows.astype(jnp.float32) * key_rows.shape[-1] ** (-0.5)
    summed = jnp.cumsum(log_forget, axis=-1)
    forget_total = summed[:, -1]
    log_weight = forget_total[:, None] - summed + input_gate
    running_max = jnp.max(log_weight, axis=-1)
    weights = jnp.exp(log_weight - running_max[:, None])
    memory = jnp.einsum(
        "bse,bsd->bed",
        weights[:, :, None] * value_rows.astype(jnp.float32),
        key_wide,
        precision=exact_mode,
    )
    normalizer = jnp.einsum("bs,bsd->bd", weights, key_wide, precision=exact_mode)
    return (memory, normalizer, running_max, forget_total)


def combine(earlier, latter):
    early_memory, early_norm, early_max, early_total = earlier
    late_memory, late_norm, late_max, late_total = latter
    joint_max = jnp.maximum(early_max + late_total, late_max)
    early_scale = jnp.exp(early_max + late_total - joint_max)
    late_scale = jnp.exp(late_max - joint_max)
    memory = early_scale[:, None, None] * early_memory + late_scale[:, None, None] * late_memory
    normalizer = early_scale[:, None] * early_norm + late_scale[:, None] * late_norm
    return (memory, normalizer, joint_max, early_total + late_total)


def span_sweep(
    query_rows, key_rows, value_rows, input_gate, log_forget, memory, normalizer, stabilizer, span
):
    block_count = query_rows.shape[1] // span

    def to_blocks(array):
        shaped = array.reshape((array.shape[0], block_count, span) + array.shape[2:])
        return jnp.moveaxis(shaped, 1, 0)

    def advance(carried, pieces):
        query_blk, key_blk, value_blk, gate_blk, forget_blk = pieces
        result = block_output(
            query_blk, key_blk, value_blk, gate_blk, forget_blk, carried[0], carried[1], carried[2]
        )
        return (combine(carried, block_summary(key_blk, value_blk, gate_blk, forget_blk)), result)

    initial = (memory, normalizer, stabilizer, jnp.zeros_like(stabilizer))
    ignored, outputs = lax.scan(
        advance,
        initial,
        tuple(
            (
                to_blocks(array)
                for array in (query_rows, key_rows, value_rows, input_gate, log_forget)
            )
        ),
    )
    return jnp.moveaxis(outputs, 0, 1).reshape(query_rows.shape[:2] + (value_rows.shape[2],))


def reverse_time(array):
    return jnp.flip(array, axis=1)


def to_heads(matrix, head_count):
    shaped = matrix.reshape(matrix.shape[0], head_count, matrix.shape[1] // head_count)
    return shaped.transpose(1, 0, 2)


def pool_window(padded, positions, channels, seq_len, group_size):
    row_count = positions.shape[0]
    group_index = channels // group_size
    reach_left = jnp.left_shift(jnp.ones_like(group_index), group_index)
    reach_right = reach_left - 1
    window_sum = jnp.zeros((row_count, channels.shape[0]), jnp.float32)
    for offset in range(-HALO, HALO):
        inside = ((offset >= -reach_left) & (offset <= reach_right)).astype(jnp.float32)
        window_sum = window_sum + inside * padded[HALO + offset : HALO + offset + row_count]
    first_pos = jnp.maximum(positions[:, None] - reach_left[None, :], 0)
    last_pos = jnp.minimum(positions[:, None] + reach_right[None, :], seq_len - 1)
    counted = (last_pos - first_pos + 1).astype(jnp.float32)
    centre = padded[HALO : HALO + row_count]
    return (window_sum / counted - centre).astype(jnp.bfloat16)


def per_device(
    tokens,
    norm_gain,
    query_weight,
    key_weight,
    value_weight,
    outgate_weight,
    gate_weight,
    gate_bias,
    decay_extra,
    init_memory,
    init_normalizer,
    head_gain,
    pool_weight,
    mem_out_weight,
    pool_out_weight,
):
    block_len = tokens.shape[1]
    model_width = tokens.shape[2]
    head_count, head_width = head_gain.shape
    span = math.gcd(block_len, 256)
    flattened = tokens[0].astype(jnp.float32)
    normed = (
        flattened
        * lax.rsqrt(jnp.mean(flattened * flattened, axis=-1, keepdims=True) + norm_eps)
        * norm_gain
    ).astype(jnp.bfloat16)
    zero_start = tuple(
        (
            jnp.zeros((block_len, weight.shape[1]), jnp.float32)
            for weight in (query_weight, key_weight, value_weight, outgate_weight, pool_weight)
        )
    )
    zero_start = zero_start + (
        jnp.zeros((model_width, mem_out_weight.shape[1]), jnp.bfloat16),
        jnp.zeros((model_width, pool_out_weight.shape[1]), jnp.bfloat16),
    )
    line_query, line_key, line_value, line_outgate, line_pool, line_mem_out, line_pool_out = (
        lax.all_gather(query_weight, "fs", axis=0, tiled=True),
        lax.all_gather(key_weight, "fs", axis=0, tiled=True),
        lax.all_gather(value_weight, "fs", axis=0, tiled=True),
        lax.all_gather(outgate_weight, "fs", axis=0, tiled=True),
        lax.all_gather(pool_weight, "fs", axis=0, tiled=True),
        lax.all_gather(mem_out_weight, "fs", axis=0, tiled=True),
        lax.all_gather(pool_out_weight, "fs", axis=0, tiled=True),
    )
    pieces = (
        lax.all_gather(line_query, "sp", axis=0, tiled=True),
        lax.all_gather(line_key, "sp", axis=0, tiled=True),
        lax.all_gather(line_value, "sp", axis=0, tiled=True),
        lax.all_gather(line_outgate, "sp", axis=0, tiled=True),
        lax.all_gather(line_pool, "sp", axis=0, tiled=True),
        lax.all_gather(line_mem_out, "sp", axis=0, tiled=True),
        lax.all_gather(line_pool_out, "sp", axis=0, tiled=True),
    )
    partial_sums = tuple(
        (
            jnp.dot(normed, weight_rows, preferred_element_type=jnp.float32)
            for weight_rows in pieces[:5]
        )
    )
    collected = tuple((weight_rows for weight_rows in pieces[5:]))
    folded = partial_sums + collected
    query_proj, key_proj, value_proj, outgate, pool_input = tuple(
        (running.astype(jnp.bfloat16) for running in folded[:5])
    )
    mem_weight_all = folded[5]
    pool_weight_all = folded[6]
    gate_pre = lax.dot_general(
        normed,
        gate_weight.reshape(4 * head_count, model_width),
        (((1,), (1,)), ((), ())),
        preferred_element_type=jnp.float32,
    ) + gate_bias.reshape(4 * head_count)
    gate_pre = gate_pre.reshape(block_len, 4, head_count).transpose(1, 2, 0)
    query_heads = to_heads(query_proj, head_count)
    key_heads = to_heads(key_proj, head_count)
    value_heads = to_heads(value_proj, head_count)
    forward_forget = jax.nn.log_sigmoid(gate_pre[1]) + decay_extra[0, 0]
    backward_forget = jax.nn.log_sigmoid(gate_pre[3]) + decay_extra[0, 1]
    zero_rows = jnp.zeros((head_count,), jnp.float32)
    identity = (
        jnp.zeros((head_count, head_width, head_width), jnp.float32),
        jnp.zeros((head_count, head_width), jnp.float32),
        jnp.full((head_count,), -1e30, jnp.float32),
        zero_rows,
    )
    front_memory, front_norm, front_max, front_total = block_summary(
        key_heads, value_heads, gate_pre[0], forward_forget
    )
    prefix = carried_in(
        (front_memory, front_norm, front_max, front_total), "sp", combine, identity, False
    )
    incoming = combine((init_memory[0, 0], init_normalizer[0, 0], zero_rows, zero_rows), prefix)
    forward_out = span_sweep(
        query_heads,
        key_heads,
        value_heads,
        gate_pre[0],
        forward_forget,
        incoming[0],
        incoming[1],
        incoming[2],
        span,
    )
    back_query = reverse_time(query_heads)
    back_key = reverse_time(key_heads)
    back_value = reverse_time(value_heads)
    back_gate = reverse_time(gate_pre[2])
    back_forget = reverse_time(backward_forget)
    rear_memory, rear_norm, rear_max, rear_total = block_summary(
        back_key, back_value, back_gate, back_forget
    )
    suffix = carried_in(
        (rear_memory, rear_norm, rear_max, rear_total), "sp", combine, identity, True
    )
    back_incoming = combine(
        (init_memory[0, 1], init_normalizer[0, 1], zero_rows, zero_rows), suffix
    )
    backward_out = reverse_time(
        span_sweep(
            back_query,
            back_key,
            back_value,
            back_gate,
            back_forget,
            back_incoming[0],
            back_incoming[1],
            back_incoming[2],
            span,
        )
    )
    summed_dirs = (forward_out + backward_out).transpose(1, 0, 2)
    normed_heads = (
        summed_dirs
        * lax.rsqrt(jnp.mean(summed_dirs * summed_dirs, axis=-1, keepdims=True) + norm_eps)
        * head_gain
    )
    out_gate = jax.nn.sigmoid(
        outgate.astype(jnp.float32).reshape(block_len, head_count, head_width)
    )
    memory_out = (
        (normed_heads * out_gate).astype(jnp.bfloat16).reshape(block_len, head_count * head_width)
    )
    padded = padded_2(pool_input, (("sp", 0),), HALO).astype(jnp.float32)
    feature_count = pool_input.shape[1]
    positions = lax.axis_index("sp") * block_len + jnp.arange(block_len, dtype=jnp.int32)
    channels = lax.axis_index("tp") * feature_count + jnp.arange(feature_count, dtype=jnp.int32)
    pool_out = pool_window(
        padded, positions, channels, block_len * lax.axis_size("sp"), model_width // 4
    )
    own_rows = block_len // lax.axis_size("tp")
    result = lax.dot_general(
        memory_out, mem_weight_all, (((1,), (1,)), ((), ())), preferred_element_type=jnp.float32
    )
    mixed = lax.psum_scatter(
        (
            result
            + lax.dot_general(
                pool_out,
                pool_weight_all,
                (((1,), (1,)), ((), ())),
                preferred_element_type=jnp.float32,
            )
        ).astype(jnp.bfloat16),
        "tp",
        scatter_dimension=0,
        tiled=True,
    )
    return mixed.reshape(1, own_rows, model_width)


def solution(mesh):
    placed = (
        P("fs", "sp", None),
        P(),
        P(("sp", "fs"), "tp"),
        P(("sp", "fs"), "tp"),
        P(("sp", "fs"), "tp"),
        P(("sp", "fs"), "tp"),
        P(None, "tp", None),
        P(None, "tp"),
        P("fs", None, "tp", "sp"),
        P("fs", None, "tp", None, None),
        P("fs", None, "tp", None),
        P("tp", None),
        P(("sp", "fs"), "tp"),
        P(("sp", "fs"), "tp"),
        P(("sp", "fs"), "tp"),
    )
    return jax.shard_map(
        per_device,
        mesh=mesh,
        in_specs=placed,
        out_specs=P("fs", ("sp", "tp"), None),
        check_vma=False,
    )
```

profile of v0, /device:TPU:0, one launch (start us, length us, event | category | flops | bytes accessed | tf_op | source)
XLA Modules:
  0.0 544.0 jit_solution(11762868126986876266)
XLA Ops:
  6.5 13.3 %all_gather.89 = bf16[512,512]{1,0:T(8,128)(2,1)} all-gather(bf16[128,512]{1,0:T(8,128)(2,1)} %param.22), channel_id=1, replica_groups=mesh['sp'=4,'fs'=4,'tp'=2] {'fs'}, dimensions={0}, use_global_device_ids=true | all-gather | bytes 655360 | tf_op jit(solution)/shard_map/all_gather | solution.py:199
  19.9 11.6 %all_gather.87 = bf16[512,512]{1,0:T(8,128)(2,1)} all-gather(bf16[128,512]{1,0:T(8,128)(2,1)} %param.23), channel_id=1, replica_groups=mesh['sp'=4,'fs'=4,'tp'=2] {'fs'}, dimensions={0}, use_global_device_ids=true | all-gather | bytes 655360 | tf_op jit(solution)/shard_map/all_gather | solution.py:200
  32.9 10.5 %all_gather.95 = bf16[512,512]{1,0:T(8,128)(2,1)} all-gather(bf16[128,512]{1,0:T(8,128)(2,1)S(1)} %copy-done.3), channel_id=1, replica_groups=mesh['sp'=4,'fs'=4,'tp'=2] {'fs'}, dimensions={0}, use_global_device_ids=true | all-gather | bytes 655360 | tf_op jit(solution)/shard_map/all_gather | solution.py:198
  43.5 10.5 %all_gather.104 = bf16[512,512]{1,0:T(8,128)(2,1)} all-gather(bf16[128,512]{1,0:T(8,128)(2,1)S(1)} %copy-done.4), channel_id=1, replica_groups=mesh['sp'=4,'fs'=4,'tp'=2] {'fs'}, dimensions={0}, use_global_device_ids=true | all-gather | bytes 655360 | tf_op jit(solution)/shard_map/all_gather | solution.py:201
  57.2 8.7 %all-gather.24.cloned.1.call-done = bf16[2048,512]{1,0:T(8,128)(2,1)} async-done(((bf16[512,512]{1,0:T(8,128)(2,1)}), bf16[2048,512]{1,0:T(8,128)(2,1)}) %all-gather.24.cloned.1.call-update) | async-done | bytes 2097168 | tf_op jit(solution)/shard_map/all_gather | solution.py:208
  68.3 43.7 %all-gather.22.cloned.1.call-done = bf16[2048,512]{1,0:T(8,128)(2,1)} async-done(((bf16[512,512]{1,0:T(8,128)(2,1)}), bf16[2048,512]{1,0:T(8,128)(2,1)}) %all-gather.22.cloned.1.call-update) | async-done | bytes 2097168 | tf_op jit(solution)/shard_map/all_gather | solution.py:209
  121.5 17.7 %all-gather.32.cloned.1.call-done = bf16[512,1024]{1,0:T(8,128)(2,1)} async-done(((bf16[128,1024]{1,0:T(8,128)(2,1)}), bf16[512,1024]{1,0:T(8,128)(2,1)}) %all-gather.32.cloned.1.call-update) | async-done | bytes 1048592 | tf_op jit(solution)/shard_map/all_gather | solution.py:202
  139.3 28.2 %all-gather.36.cloned.1.call-done = bf16[512,1024]{1,0:T(8,128)(2,1)} async-done(((bf16[128,1024]{1,0:T(8,128)(2,1)}), bf16[512,1024]{1,0:T(8,128)(2,1)}) %all-gather.36.cloned.1.call-update) | async-done | bytes 1048592 | tf_op jit(solution)/shard_map/all_gather | solution.py:204
  167.5 10.6 %all_gather.106 = bf16[512,512]{1,0:T(8,128)(2,1)} all-gather(bf16[128,512]{1,0:T(8,128)(2,1)S(1)} %copy-done.5), channel_id=1, replica_groups=mesh['sp'=4,'fs'=4,'tp'=2] {'fs'}, dimensions={0}, use_global_device_ids=true | all-gather | bytes 655360 | tf_op jit(solution)/shard_map/all_gather | solution.py:203
  185.9 12.3 %all-reduce.4 = (f32[16]{0:T(128)S(1)}, f32[16]{0:T(128)S(1)}, f32[16]{0:T(128)S(1)}, f32[16]{0:T(128)S(1)}) all-reduce(f32[16]{0:T(128)S(1)} %dynamic-update-slice.2, f32[16]{0:T(128)S(1)} %dynamic-update-slice.3, f32[16]{0:T(128)S(1)} %dynamic-update-slice, f32[16]{0:T(128)S(1)} %dynamic-update-slice.1), channel_id=6, replica_groups=mesh['sp'=4,'fs'=4,'tp'=2] {'sp'}, use_global_device_ids=true, to_apply=%add.2 | all-reduce | flops 64 | bytes 512
  201.4 12.5 %all-gather.8 = f32[4,4,128]{2,1,0:T(4,128)S(1)} all-gather(f32[1,4,128]{2,1,0:T(4,128)S(1)} %bitcast.306), channel_id=5, replica_groups=mesh['sp'=4,'fs'=4,'tp'=2] {'sp'}, dimensions={0}, use_global_device_ids=true | all-gather | bytes 10240 | tf_op jit(solution)/shard_map/all_gather | solution.py:17
  214.2 12.1 %all-gather.9 = f32[4,4,128]{2,1,0:T(4,128)S(1)} all-gather(f32[1,4,128]{2,1,0:T(4,128)S(1)} %bitcast.302), channel_id=9, replica_groups=mesh['sp'=4,'fs'=4,'tp'=2] {'sp'}, dimensions={0}, use_global_device_ids=true | all-gather | bytes 10240 | tf_op jit(solution)/shard_map/all_gather | solution.py:17
  229.1 31.8 %all-gather.28.cloned.1.call-done = bf16[2048,512]{1,0:T(8,128)(2,1)} async-done(((bf16[512,512]{1,0:T(8,128)(2,1)}), bf16[2048,512]{1,0:T(8,128)(2,1)}) %all-gather.28.cloned.1.call-update) | async-done | bytes 2097168 | tf_op jit(solution)/shard_map/all_gather | solution.py:210
  265.4 23.9 %all-gather.40.cloned.1.call-done = f32[16,128,128]{2,1,0:T(8,128)} async-done(((f32[4,128,128]{2,1,0:T(8,128)}), f32[16,128,128]{2,1,0:T(8,128)}) %all-gather.40.cloned.1.call-update) | async-done | bytes 1048592 | tf_op jit(solution)/shard_map/all_gather | solution.py:17
  289.3 7.4 %while.12 = (s32[]{:T(128)}, f32[4,128,128]{2,1,0:T(8,128)S(1)}, f32[4,128]{1,0:T(4,128)S(1)}, f32[4]{0:T(128)S(1)}, f32[4]{0:T(128)S(1)}, /*index=5*/s32[]{:T(1...) while((s32[]{:T(128)}, f32[4,128,128]{2,1,0:T(8,128)S(1)}, ...), condition=%wide.region_5.6_spmd.clone, body=%wide.region_4.5_spmd.clone.sunk | while | flops 330284 | bytes 792973 | solution.py:28
  300.1 18.2 %all-gather.42.cloned.1.call-done = f32[16,128,128]{2,1,0:T(8,128)} async-done(((f32[4,128,128]{2,1,0:T(8,128)}), f32[16,128,128]{2,1,0:T(8,128)}) %all-gather.42.cloned.1.call-update) | async-done | bytes 1048592 | tf_op jit(solution)/shard_map/all_gather | solution.py:17
  318.3 7.5 %while.13 = (s32[]{:T(128)}, f32[4,128,128]{2,1,0:T(8,128)S(1)}, f32[4,128]{1,0:T(4,128)S(1)}, f32[4]{0:T(128)S(1)}, f32[4]{0:T(128)S(1)}, /*index=5*/s32[]{:T(1...) while((s32[]{:T(128)}, f32[4,128,128]{2,1,0:T(8,128)S(1)}, ...), condition=%wide.region_12.13_spmd.clone, body=%wide.region_11.12_spmd.clone.sunk | while | flops 330288 | bytes 793035 | solution.py:28
  329.0 5.0 rev.26
  336.1 63.9 %all-gather.34.cloned.1.call-done = bf16[2048,1024]{1,0:T(8,128)(2,1)} async-done(((bf16[512,1024]{1,0:T(8,128)(2,1)}), bf16[2048,1024]{1,0:T(8,128)(2,1)}) %all-gather.34.cloned.1.call-update) | async-done | bytes 4194320 | tf_op jit(solution)/shard_map/all_gather | solution.py:211
  406.4 4.2 collective-permute-done.1
  410.8 69.9 %all-gather.38.cloned.1.call-done = bf16[2048,1024]{1,0:T(8,128)(2,1)} async-done(((bf16[512,1024]{1,0:T(8,128)(2,1)}), bf16[2048,1024]{1,0:T(8,128)(2,1)}) %all-gather.38.cloned.1.call-update) | async-done | bytes 4194320 | tf_op jit(solution)/shard_map/all_gather | solution.py:213
  480.8 5.3 fusion.74
  486.1 40.3 %all-gather.30.cloned.1.call-done = bf16[2048,512]{1,0:T(8,128)(2,1)} async-done(((bf16[512,512]{1,0:T(8,128)(2,1)}), bf16[2048,512]{1,0:T(8,128)(2,1)}) %all-gather.30.cloned.1.call-update) | async-done | bytes 2097168 | tf_op jit(solution)/shard_map/all_gather | solution.py:212
  529.8 7.3 %reduce-scatter.2.cloned.1.call-done = bf16[128,2048]{1,0:T(8,128)(2,1)} async-done(((bf16[256,2048]{1,0:T(8,128)(2,1)}), bf16[128,2048]{1,0:T(8,128)(2,1)}) %reduce-scatter.2.cloned.1.call-update) | async-done | bytes 524304 | tf_op jit(solution)/shard_map/reduce_scatter | solution.py:315
  (244 shorter events, 67.3 us)
Async XLA Ops:
  6.5 59.4 %all-gather.24.cloned.1.call-start = ((), (), s32[]{:S(2)}) async-start(), calls=%async_computation.2 | async-start | bytes 2621440 | tf_op jit(solution)/shard_map/all_gather | solution.py:208
  19.9 92.1 %all-gather.22.cloned.1.call-start = ((), (), s32[]{:S(2)}) async-start(), calls=%async_computation.1 | async-start | bytes 2621440 | tf_op jit(solution)/shard_map/all_gather | solution.py:209
  31.5 107.7 %all-gather.32.cloned.1.call-start = ((), (), s32[]{:S(2)}) async-start(), calls=%async_computation.6 | async-start | bytes 1310720 | tf_op jit(solution)/shard_map/all_gather | solution.py:202
  32.3 135.2 %all-gather.36.cloned.1.call-start = ((), (), s32[]{:S(2)}) async-start(), calls=%async_computation.8 | async-start | bytes 1310720 | tf_op jit(solution)/shard_map/all_gather | solution.py:204
  32.8 193.5 %all-gather.26.cloned.1.call-start = ((), (), s32[]{:S(2)}) async-start(), calls=%async_computation.3 | async-start | bytes 2621440 | tf_op jit(solution)/shard_map/all_gather | solution.py:207
  43.5 217.5 %all-gather.28.cloned.1.call-start = ((), (), s32[]{:S(2)}) async-start(), calls=%async_computation.4 | async-start | bytes 2621440 | tf_op jit(solution)/shard_map/all_gather | solution.py:210
  54.1 235.2 %all-gather.40.cloned.1.call-start = ((), (), s32[]{:S(2)}) async-start(), calls=%async_computation.11 | async-start | bytes 1310720 | tf_op jit(solution)/shard_map/all_gather | solution.py:17
  54.6 206.3 %copy-start.30 = (f32[256]{0:T(256)}, f32[256]{0:T(256)S(1)}, u32[]{:S(2)}) copy-start(f32[256]{0:T(256)S(1)} %add_rsqrt_fusion.1) | copy-start | bytes 3076
  68.3 132.7 %copy-start.2 = (bf16[32,4,8,128]{3,2,1,0:T(8,128)(2,1)}, bf16[32,4,8,128]{3,2,1,0:T(8,128)(2,1)S(1)}, u32[]{:S(2)}) copy-start(bf16[32,4,8,128]{3,2,1,0:T(8,128)(2,1)S(1)} %fusion.36) | copy-start | bytes 786436
  116.2 202.0 %all-gather.42.cloned.1.call-start = ((), (), s32[]{:S(2)}) async-start(), calls=%async_computation.12 | async-start | bytes 1310720 | tf_op jit(solution)/shard_map/all_gather | solution.py:17
  121.4 278.6 %all-gather.34.cloned.1.call-start = ((), (), s32[]{:S(2)}) async-start(), calls=%async_computation.7 | async-start | bytes 5242880 | tf_op jit(solution)/shard_map/all_gather | solution.py:211
  139.2 341.4 %all-gather.38.cloned.1.call-start = ((), (), s32[]{:S(2)}) async-start(), calls=%async_computation.9 | async-start | bytes 5242880 | tf_op jit(solution)/shard_map/all_gather | solution.py:213
  167.5 358.9 %all-gather.30.cloned.1.call-start = ((), (), s32[]{:S(2)}) async-start(), calls=%async_computation.5 | async-start | bytes 2621440 | tf_op jit(solution)/shard_map/all_gather | solution.py:212
  178.2 359.0 %reduce-scatter.2.cloned.1.call-start = ((), (), s32[]{:S(2)}) async-start(), calls=%async_computation.10 | async-start | bytes 1572864 | tf_op jit(solution)/shard_map/reduce_scatter | solution.py:315
  403.5 77.2 %copy-start.9 = (s32[1024]{0:T(1024)S(1)}, s32[1024]{0:T(1024)}, u32[]{:S(2)}) copy-start(s32[1024]{0:T(1024)} %get-tuple-element.635) | copy-start | bytes 12292
  403.5 77.2 %copy-start.10 = (s32[1024]{0:T(1024)S(1)}, s32[1024]{0:T(1024)}, u32[]{:S(2)}) copy-start(s32[1024]{0:T(1024)} %get-tuple-element.636) | copy-start | bytes 12292
  403.5 77.2 %copy-start.11 = (f32[1024]{0:T(1024)S(1)}, f32[1024]{0:T(1024)}, u32[]{:S(2)}) copy-start(f32[1024]{0:T(1024)} %get-tuple-element.637) | copy-start | bytes 12292
  403.5 77.2 %copy-start.12 = (f32[1024]{0:T(1024)S(1)}, f32[1024]{0:T(1024)}, u32[]{:S(2)}) copy-start(f32[1024]{0:T(1024)} %get-tuple-element.638) | copy-start | bytes 12292
  403.5 77.2 %copy-start.13 = (f32[1024]{0:T(1024)S(1)}, f32[1024]{0:T(1024)}, u32[]{:S(2)}) copy-start(f32[1024]{0:T(1024)} %get-tuple-element.639) | copy-start | bytes 12292
  403.5 77.2 %copy-start.14 = (f32[1024]{0:T(1024)S(1)}, f32[1024]{0:T(1024)}, u32[]{:S(2)}) copy-start(f32[1024]{0:T(1024)} %get-tuple-element.640) | copy-start | bytes 12292
  403.5 77.2 %copy-start.15 = (f32[1024]{0:T(1024)S(1)}, f32[1024]{0:T(1024)}, u32[]{:S(2)}) copy-start(f32[1024]{0:T(1024)} %get-tuple-element.641) | copy-start | bytes 12292
  403.5 77.2 %copy-start.16 = (f32[1024]{0:T(1024)S(1)}, f32[1024]{0:T(1024)}, u32[]{:S(2)}) copy-start(f32[1024]{0:T(1024)} %get-tuple-element.642) | copy-start | bytes 12292
  403.7 2.8 collective-permute-start
  405.0 5.7 %collective-permute-start.1 = (bf16[8,1024]{1,0:T(8,128)(2,1)S(1)}, bf16[8,1024]{1,0:T(8,128)(2,1)S(1)}, u32[]{:S(2)}, u32[]{:S(2)}) collective-permute-start(bf16[8,1024]{1,0:T(8,128)(2,1)S(1)} %get-tuple-element.621), channel_id=1, source_target_pairs={{8,0},{16,8},{24,16},{9,1},{17,9},{25,17},{10,2},{18,10},{26,18},{... | collective-permute-start | bytes 49160 | tf_op jit(solution)/shard_map/ppermute | solution.py:39
  (29 other events, 1408.9 us)
Sparse Core Ops, SparseCore 0:
  20.0 45.9 all-gather.23
  67.5 44.4 all-gather.21
  113.8 25.3 all-gather.31
  140.9 26.4 all-gather.35
  168.9 46.0 all-gather.25
  216.4 44.4 all-gather.27
  262.5 26.7 all-gather.39
  290.9 27.3 all-gather.41
  319.8 80.1 all-gather.33
  401.4 79.2 all-gather.37
  482.2 44.1 all-gather.29
  529.9 7.1 reduce-scatter.1
where the time goes:
time: 545 us; the launch traced here: 544 us
  waiting for transfers between devices  359 us (66%)
  blocking collectives  93.4 us (17%)
  matrix products  34.2 us (6%)
  other arithmetic  26.8 us (5%)
  between operations  15 us (3%)
  local copies, waits for them, and re-layouts  12.1 us (2%)
    all_gather x1, waiting for transfers between devices, per_device(): lax.all_gather(line_pool_out, 'sp', axis=0, tiled=True)  69.9 us
    all_gather x1, waiting for transfers between devices, per_device(): lax.all_gather(line_pool, 'sp', axis=0, tiled=True)  63.9 us
    all_gather x1, waiting for transfers between devices, per_device(): lax.all_gather(line_value, 'sp', axis=0, tiled=True)  43.7 us
    all_gather x2, waiting for transfers between devices, carried_in(): everything = jax.tree.map(lambda part: lax.all_gather(part, axis), x)  42.1 us
    all_gather x1, waiting for transfers between devices, per_device(): lax.all_gather(line_mem_out, 'sp', axis=0, tiled=True)  40.3 us
    all_gather x1, waiting for transfers between devices, per_device(): lax.all_gather(line_outgate, 'sp', axis=0, tiled=True)  31.8 us
    all_gather x1, waiting for transfers between devices, per_device(): lax.all_gather(pool_out_weight, 'fs', axis=0, tiled=True)  28.2 us
    all_gather x2, blocking collectives, carried_in(): everything = jax.tree.map(lambda part: lax.all_gather(part, axis), x)  24.6 us
  transfers between devices with their start and end apart: 14, of which 12 were waited for; matrix products, arithmetic and copies ran while one was open for 13% of the time, Pallas kernels for 0%

commit v1 on v0

--- a/solution.py
+++ b/solution.py
@@ -1,9 +1,14 @@
+import functools
 import math
 
 import jax
 import jax.numpy as jnp
 from jax import lax
+from jax.experimental import pallas as pl
+from jax.experimental.pallas import tpu as pltpu
 from jax.sharding import PartitionSpec as P
+
+MESH = pl.DeviceIdType.MESH
 
 HALO = 8
 
@@ -329,6 +334,498 @@
     return mixed.reshape(1, own_rows, model_width)
 
 
+def aligned(start, size):
+    return pl.ds(pl.multiple_of(start, size), size)
+
+
+def gather_kernel(n_sp, n_fs, widths, *refs):
+    count = len(widths)
+    token_ref, decay_ref = refs[:2]
+    weight_refs = refs[2 : 2 + count]
+    x_ref, decay_out, in_ref, out_ref = refs[2 + count : 6 + count]
+    (
+        local_sem,
+        token_local,
+        weight_send,
+        weight_recv,
+        decay_send,
+        decay_recv,
+        token_send,
+        token_recv,
+        swap_send,
+        swap_recv,
+        row_send,
+        row_recv,
+    ) = refs[6 + count :]
+    sp, fs, tp = (lax.axis_index(name) for name in ("sp", "fs", "tp"))
+    other = 1 - tp
+    rows = weight_refs[0].shape[0]
+    block = token_ref.shape[0]
+    half = block // 2
+    ups = [lax.rem(sp + k, n_sp) for k in range(n_sp)]
+    downs = [lax.rem(sp + n_sp - k, n_sp) for k in range(n_sp)]
+    fs_up = [lax.rem(fs + j, n_fs) for j in range(n_fs)]
+    fs_down = [lax.rem(fs + n_fs - j, n_fs) for j in range(n_fs)]
+
+    barrier = pltpu.get_barrier_semaphore()
+    for k in range(1, n_sp):
+        pl.semaphore_signal(barrier, inc=1, device_id={"sp": ups[k]}, device_id_type=MESH)
+    for j in range(1, n_fs):
+        pl.semaphore_signal(barrier, inc=1, device_id={"fs": fs_up[j]}, device_id_type=MESH)
+    pl.semaphore_signal(barrier, inc=1, device_id={"tp": other}, device_id_type=MESH)
+    pl.semaphore_wait(barrier, n_sp + n_fs - 1)
+
+    in_count = count - 2
+    in_width = sum(widths[:in_count])
+
+    def landing(i, source_sp):
+        at = aligned((source_sp * n_fs + fs) * rows, rows)
+        start = sum(widths[:i])
+        if i < in_count:
+            return in_ref.at[at, pl.ds(start, widths[i])]
+        return out_ref.at[at, pl.ds(start - in_width, widths[i])]
+
+    def piece(i, target_sp):
+        return weight_refs[i].at[:, aligned(target_sp * widths[i], widths[i])]
+
+    locals_ = []
+    for i in range(count):
+        locals_.append(pltpu.make_async_copy(piece(i, sp), landing(i, sp), local_sem.at[i]))
+    for copy in locals_:
+        copy.start()
+    own_tokens = pltpu.make_async_copy(
+        token_ref, x_ref.at[aligned(sp * block, block)], token_local.at[0]
+    )
+    own_tokens.start()
+    own_decay = pltpu.make_async_copy(decay_ref.at[sp], decay_out.at[sp], token_local.at[1])
+    own_decay.start()
+
+    def weight_copy(i, k, target, source):
+        return pltpu.make_async_remote_copy(
+            src_ref=piece(i, target),
+            dst_ref=landing(i, source),
+            send_sem=weight_send.at[k - 1, i],
+            recv_sem=weight_recv.at[k - 1, i],
+            device_id={"sp": target},
+            device_id_type=MESH,
+        )
+
+    def decay_copy(k, target, source):
+        return pltpu.make_async_remote_copy(
+            src_ref=decay_ref.at[target],
+            dst_ref=decay_out.at[source],
+            send_sem=decay_send.at[k - 1],
+            recv_sem=decay_recv.at[k - 1],
+            device_id={"sp": target},
+            device_id_type=MESH,
+        )
+
+    def token_copy(k, target, source):
+        return pltpu.make_async_remote_copy(
+            src_ref=token_ref.at[aligned(tp * half, half)],
+            dst_ref=x_ref.at[aligned(source * block + tp * half, half)],
+            send_sem=token_send.at[k - 1],
+            recv_sem=token_recv.at[k - 1],
+            device_id={"sp": target},
+            device_id_type=MESH,
+        )
+
+    def swap_copy(k, side):
+        at = x_ref.at[aligned(downs[k] * block + side * half, half)]
+        return pltpu.make_async_remote_copy(
+            src_ref=at,
+            dst_ref=at,
+            send_sem=swap_send.at[k - 1],
+            recv_sem=swap_recv.at[k - 1],
+            device_id={"tp": other},
+            device_id_type=MESH,
+        )
+
+    def row_copies(k, j, at_fs):
+        at = aligned((downs[k] * n_fs + at_fs) * rows, rows)
+        made = []
+        for which, ref in enumerate((in_ref, out_ref)):
+            made.append(
+                pltpu.make_async_remote_copy(
+                    src_ref=ref.at[at],
+                    dst_ref=ref.at[at],
+                    send_sem=row_send.at[k, j - 1, which],
+                    recv_sem=row_recv.at[k, j - 1, which],
+                    device_id={"fs": fs_up[j]},
+                    device_id_type=MESH,
+                )
+            )
+        return made
+
+    for k in range(1, n_sp):
+        for i in range(count):
+            weight_copy(i, k, ups[k], sp).start()
+    for k in range(1, n_sp):
+        decay_copy(k, ups[k], sp).start()
+        token_copy(k, ups[k], sp).start()
+    for copy in locals_:
+        copy.wait()
+    for k in range(n_sp):
+        if k:
+            for i in range(count):
+                weight_copy(i, k, ups[k], downs[k]).wait_recv()
+        for j in range(1, n_fs):
+            for copy in row_copies(k, j, fs):
+                copy.start()
+    for k in range(1, n_sp):
+        token_copy(k, ups[k], downs[k]).wait_recv()
+        swap_copy(k, tp).start()
+    own_tokens.wait()
+    own_decay.wait()
+    for k in range(1, n_sp):
+        decay_copy(k, ups[k], downs[k]).wait_recv()
+        swap_copy(k, other).wait_recv()
+    for k in range(n_sp):
+        for j in range(1, n_fs):
+            for copy in row_copies(k, j, fs_down[j]):
+                copy.wait_recv()
+    for k in range(1, n_sp):
+        for i in range(count):
+            weight_copy(i, k, ups[k], sp).wait_send()
+        decay_copy(k, ups[k], sp).wait_send()
+        token_copy(k, ups[k], sp).wait_send()
+        swap_copy(k, tp).wait_send()
+    for k in range(n_sp):
+        for j in range(1, n_fs):
+            for copy in row_copies(k, j, fs):
+                copy.wait_send()
+
+
+def gather_all(tokens, decay, weights):
+    n_sp, n_fs = lax.axis_size("sp"), lax.axis_size("fs")
+    widths = tuple(weight.shape[1] // n_sp for weight in weights)
+    block, model_width = tokens.shape
+    count = len(weights)
+    vmem = pl.BlockSpec(memory_space=pltpu.VMEM)
+    dma = pltpu.SemaphoreType.DMA
+    return pl.pallas_call(
+        functools.partial(gather_kernel, n_sp, n_fs, widths),
+        out_shape=(
+            jax.ShapeDtypeStruct((n_sp * block, model_width), tokens.dtype),
+            jax.ShapeDtypeStruct(decay.shape, decay.dtype),
+            jax.ShapeDtypeStruct((model_width, sum(widths[:-2])), tokens.dtype),
+            jax.ShapeDtypeStruct((model_width, sum(widths[-2:])), tokens.dtype),
+        ),
+        in_specs=[vmem] * (2 + count),
+        out_specs=(vmem,) * 4,
+        scratch_shapes=[
+            dma((count,)),
+            dma((2,)),
+            dma((n_sp - 1, count)),
+            dma((n_sp - 1, count)),
+            dma((n_sp - 1,)),
+            dma((n_sp - 1,)),
+            dma((n_sp - 1,)),
+            dma((n_sp - 1,)),
+            dma((n_sp - 1,)),
+            dma((n_sp - 1,)),
+            dma((n_sp, n_fs - 1, 2)),
+            dma((n_sp, n_fs - 1, 2)),
+        ],
+        compiler_params=pltpu.CompilerParams(
+            collective_id=0, has_side_effects=True, vmem_limit_bytes=40 * 2**20
+        ),
+        name="gather_all",
+    )(tokens, decay, *weights)
+
+
+def memory_kernel(
+    q_ref, qk_ref, k_ref, v_ref, gate_ref, cols_ref, rows_ref, mem_ref, norm_ref, gain_ref, o_ref
+):
+    tb = q_ref.shape[0]
+    seq = k_ref.shape[0]
+    width = q_ref.shape[1]
+    scale = width ** (-0.5)
+    q = q_ref[...]
+    cols = cols_ref[...]
+    front_peak, rear_peak = cols[:, 0:1], cols[:, 1:2]
+    front_max, rear_max = cols[:, 2:3], cols[:, 3:4]
+    rear_own = cols[:, 4:5]
+    score = (
+        lax.dot_general(
+            q, k_ref[...], (((1,), (1,)), ((), ())), preferred_element_type=jnp.float32
+        )
+        * scale
+    )
+    t = pl.program_id(0) * tb + lax.broadcasted_iota(jnp.int32, (tb, seq), 0)
+    s = lax.broadcasted_iota(jnp.int32, (tb, seq), 1)
+    front = s <= t
+    weight = (
+        jnp.exp(
+            jnp.where(front, rows_ref[0:1, :] - front_peak, rows_ref[1:2, :] - rear_peak)
+        )
+        * score
+    )
+    front_weight = jnp.where(front, weight, 0.0)
+    rear_weight = jnp.where(front, 0.0, weight)
+    wide = q.astype(jnp.float32)
+    own_score = jnp.sum(wide * qk_ref[...].astype(jnp.float32), axis=1, keepdims=True) * scale
+    own_weight = jnp.exp(rear_own - rear_peak) * own_score
+    start = t.shape[0] * pl.program_id(0)
+    own_value = v_ref[pl.ds(pl.multiple_of(start, tb), tb), :].astype(jnp.float32)
+    carry = lax.dot_general(
+        wide,
+        mem_ref[...],
+        (((1,), (1,)), ((), ())),
+        precision=exact_mode,
+        preferred_element_type=jnp.float32,
+    )
+
+    def one(direction, weights, peak, top, extra_num, extra_den):
+        decay = jnp.exp(-peak)
+        num = decay * carry[:, direction * width : (direction + 1) * width] + jnp.dot(
+            weights.astype(jnp.bfloat16), v_ref[...], preferred_element_type=jnp.float32
+        )
+        den = decay * jnp.sum(
+            wide * norm_ref[direction : direction + 1, :], axis=1, keepdims=True
+        ) + jnp.sum(weights, axis=1, keepdims=True)
+        return (num + extra_num) / jnp.maximum(jnp.abs(den + extra_den), jnp.exp(-top))
+
+    total = one(0, front_weight, front_peak, front_max, 0.0, 0.0) + one(
+        1,
+        rear_weight,
+        rear_peak,
+        rear_max,
+        own_weight.astype(jnp.bfloat16).astype(jnp.float32) * own_value,
+        own_weight,
+    )
+    normed = (
+        total
+        * lax.rsqrt(jnp.mean(total * total, axis=-1, keepdims=True) + norm_eps)
+        * gain_ref[...]
+    )
+    o_ref[...] = (normed * jax.nn.sigmoid(gate_ref[...].astype(jnp.float32))).astype(jnp.bfloat16)
+
+
+def memory_mix(proj, cols, rows, memory, normalizer, gain, width):
+    seq = proj.shape[0]
+    tb = math.gcd(seq, 256)
+
+    def part(i, whole):
+        if whole:
+            return pl.BlockSpec((seq, width), lambda t: (0, i))
+        return pl.BlockSpec((tb, width), lambda t: (t, i))
+
+    def fixed(array):
+        return pl.BlockSpec(array.shape, lambda t: (0, 0))
+
+    return pl.pallas_call(
+        memory_kernel,
+        grid=(seq // tb,),
+        out_shape=jax.ShapeDtypeStruct((seq, width), jnp.bfloat16),
+        in_specs=[
+            part(0, False),
+            part(1, False),
+            part(1, True),
+            part(2, True),
+            part(3, False),
+            pl.BlockSpec((tb, cols.shape[1]), lambda t: (t, 0)),
+            fixed(rows),
+            fixed(memory),
+            fixed(normalizer),
+            fixed(gain),
+        ],
+        out_specs=pl.BlockSpec((tb, width), lambda t: (t, 0)),
+        name="memory_mix",
+    )(proj, proj, proj, proj, proj, cols, rows, memory, normalizer, gain)
+
+
+def project_kernel(
+    n_sp, mem_ref, pool_ref, weight_ref, o_ref,
+    give, take, send, land, own, swap_send, swap_recv, z_send, z_recv,
+):
+    sp, tp = lax.axis_index("sp"), lax.axis_index("tp")
+    other = 1 - tp
+    half = o_ref.shape[0]
+    width = o_ref.shape[1]
+    split = mem_ref.shape[1]
+    tile = math.gcd(width, 512)
+
+    barrier = pltpu.get_barrier_semaphore()
+    for k in range(1, n_sp):
+        pl.semaphore_signal(
+            barrier, inc=1, device_id={"sp": lax.rem(sp + k, n_sp)}, device_id_type=MESH
+        )
+    pl.semaphore_signal(barrier, inc=1, device_id={"tp": other}, device_id_type=MESH)
+    pl.semaphore_wait(barrier, n_sp)
+
+    def product(target, side, c):
+        at = aligned(target * 2 * half + side * half, half)
+        columns = pl.ds(c * tile, tile)
+        dims = (((1,), (1,)), ((), ()))
+        return lax.dot_general(
+            mem_ref[at, :],
+            weight_ref[columns, :split],
+            dims,
+            preferred_element_type=jnp.float32,
+        ) + lax.dot_general(
+            pool_ref[at, :],
+            weight_ref[columns, split:],
+            dims,
+            preferred_element_type=jnp.float32,
+        )
+
+    def swap(k):
+        return pltpu.make_async_remote_copy(
+            src_ref=give.at[k],
+            dst_ref=take.at[k],
+            send_sem=swap_send.at[k],
+            recv_sem=swap_recv.at[k],
+            device_id={"tp": other},
+            device_id_type=MESH,
+        )
+
+    def pass_on(k):
+        return pltpu.make_async_remote_copy(
+            src_ref=send.at[k - 1],
+            dst_ref=land.at[k - 1],
+            send_sem=z_send.at[k - 1],
+            recv_sem=z_recv.at[k - 1],
+            device_id={"sp": lax.rem(sp + k, n_sp)},
+            device_id_type=MESH,
+        )
+
+    order = list(range(1, n_sp)) + [0]
+    for k in order:
+        target = lax.rem(sp + k, n_sp)
+        for c in range(width // tile):
+            give[k, :, c * tile : (c + 1) * tile] = product(target, other, c).astype(jnp.bfloat16)
+        swap(k).start()
+    for k in order:
+        target = lax.rem(sp + k, n_sp)
+        swap(k).wait_recv()
+        for c in range(width // tile):
+            at = slice(c * tile, (c + 1) * tile)
+            both = product(target, tp, c) + take[k, :, at].astype(jnp.float32)
+            if k:
+                send[k - 1, :, at] = both.astype(jnp.bfloat16)
+            else:
+                own[:, at] = both
+        if k:
+            pass_on(k).start()
+    for k in range(1, n_sp):
+        pass_on(k).wait_recv()
+        own[...] += land[k - 1].astype(jnp.float32)
+    o_ref[...] = own[...].astype(jnp.bfloat16)
+    for k in range(n_sp):
+        swap(k).wait_send()
+        if k:
+            pass_on(k).wait_send()
+
+
+def project_out(memory_out, pool_out, weight):
+    n_sp = lax.axis_size("sp")
+    half = memory_out.shape[0] // (2 * n_sp)
+    width = weight.shape[0]
+    vmem = pl.BlockSpec(memory_space=pltpu.VMEM)
+    dma = pltpu.SemaphoreType.DMA
+    buffers = pltpu.VMEM((n_sp, half, width), jnp.bfloat16)
+    fewer = pltpu.VMEM((n_sp - 1, half, width), jnp.bfloat16)
+    return pl.pallas_call(
+        functools.partial(project_kernel, n_sp),
+        out_shape=jax.ShapeDtypeStruct((half, width), jnp.bfloat16),
+        in_specs=[vmem] * 3,
+        out_specs=vmem,
+        scratch_shapes=[
+            buffers,
+            buffers,
+            fewer,
+            fewer,
+            pltpu.VMEM((half, width), jnp.float32),
+            dma((n_sp,)),
+            dma((n_sp,)),
+            dma((n_sp - 1,)),
+            dma((n_sp - 1,)),
+        ],
+        compiler_params=pltpu.CompilerParams(
+            collective_id=1, has_side_effects=True, vmem_limit_bytes=40 * 2**20
+        ),
+        name="project_out",
+    )(memory_out, pool_out, weight)
+
+
+def by_head(
+    tokens,
+    norm_gain,
+    query_weight,
+    key_weight,
+    value_weight,
+    outgate_weight,
+    gate_weight,
+    gate_bias,
+    decay_extra,
+    init_memory,
+    init_normalizer,
+    head_gain,
+    pool_weight,
+    mem_out_weight,
+    pool_out_weight,
+):
+    model_width = tokens.shape[2]
+    width = head_gain.shape[1]
+    n_sp = lax.axis_size("sp")
+    sp, tp = lax.axis_index("sp"), lax.axis_index("tp")
+    everything, decay, in_weight, out_weight = gather_all(
+        tokens[0],
+        decay_extra[0].transpose(1, 0, 2),
+        (
+            query_weight,
+            key_weight,
+            value_weight,
+            outgate_weight,
+            pool_weight,
+            mem_out_weight,
+            pool_out_weight,
+        ),
+    )
+    seq = everything.shape[0]
+    decay = decay.transpose(1, 0, 2).reshape(2, seq)
+    flattened = everything.astype(jnp.float32)
+    normed = (
+        flattened
+        * lax.rsqrt(jnp.mean(flattened * flattened, axis=-1, keepdims=True) + norm_eps)
+        * norm_gain
+    ).astype(jnp.bfloat16)
+    proj = jnp.dot(normed, in_weight, preferred_element_type=jnp.float32).astype(jnp.bfloat16)
+    own_gates = lax.dynamic_index_in_dim(gate_weight, sp, 1, keepdims=False)
+    own_bias = lax.dynamic_index_in_dim(gate_bias, sp, 1, keepdims=True)
+    gate_pre = (
+        lax.dot_general(
+            own_gates, normed, (((1,), (1,)), ((), ())), preferred_element_type=jnp.float32
+        )
+        + own_bias
+    )
+    front_sum = lax.cumsum(jax.nn.log_sigmoid(gate_pre[1]) + decay[0])
+    rear_sum = lax.cumsum(jax.nn.log_sigmoid(gate_pre[3]) + decay[1], reverse=True)
+    front_level = gate_pre[0] - front_sum
+    rear_level = gate_pre[2] - rear_sum
+    front_peak = jnp.maximum(lax.cummax(front_level), 0.0)
+    rear_peak = jnp.maximum(lax.cummax(rear_level, reverse=True), 0.0)
+    rows = jnp.stack([front_level, rear_level])
+    cols = jnp.stack(
+        [front_peak, rear_peak, front_sum + front_peak, rear_sum + rear_peak, rear_level]
+    ).T
+    memory = lax.dynamic_index_in_dim(init_memory[0], sp, 1, keepdims=False)
+    normalizer = lax.dynamic_index_in_dim(init_normalizer[0], sp, 1, keepdims=False)
+    gain = lax.dynamic_slice_in_dim(head_gain, sp, 1, 0)
+    memory_out = memory_mix(
+        proj, cols, rows, memory.reshape(2 * width, width), normalizer, gain, width
+    )
+    pool_input = proj[:, 4 * width :]
+    features = pool_input.shape[1]
+    padded = jnp.pad(pool_input.astype(jnp.float32), ((HALO, HALO), (0, 0)))
+    positions = jnp.arange(seq, dtype=jnp.int32)
+    channels = (tp * n_sp + sp) * features + jnp.arange(features, dtype=jnp.int32)
+    pool_out = pool_window(padded, positions, channels, seq, model_width // 4)
+    mixed = project_out(memory_out, pool_out, out_weight)
+    return mixed[None]
+
+
 def solution(mesh):
     placed = (
         P("fs", "sp", None),
@@ -347,8 +844,23 @@
         P(("sp", "fs"), "tp"),
         P(("sp", "fs"), "tp"),
     )
+
+    def body(*args):
+        heads, width = args[11].shape
+        features = args[12].shape[1]
+        fits = (
+            lax.axis_size("tp") == 2
+            and heads == lax.axis_size("sp")
+            and heads > 1
+            and lax.axis_size("fs") > 1
+            and width == 128
+            and features % (128 * heads) == 0
+            and args[0].shape[1] % 32 == 0
+        )
+        return (by_head if fits else per_device)(*args)
+
     return jax.shard_map(
-        per_device,
+        body,
         mesh=mesh,
         in_specs=placed,
         out_specs=P("fs", ("sp", "tp"), None),

time: 545 us -> 177 us (0.32)
  the two profiles are of different devices: /device:TPU:0 before, /device:TPU:9 now
where the time goes in v1:
time: 177 us; the launch traced here: 176 us
  Pallas kernels  138 us (78%)
  other arithmetic  15.9 us (9%)
  local copies, waits for them, and re-layouts  15.6 us (9%)
  matrix products  6.91 us (4%)
    pallas_call x1, Pallas kernels, gather_all(): pl.pallas_call(functools.partial(gather_kernel, n_sp, n_fs, widths), out_...  78.3 us
    pallas_call x1, Pallas kernels, project_out(): pl.pallas_call(functools.partial(project_kernel, n_sp), out_shape=jax.Sha...  51.9 us
    unnamed x32, local copies, waits for them, and re-layouts  10.5 us
    convert_element_type x1, other arithmetic, pool_window(): return (window_sum / counted - centre).astype(jnp.bfloat16)  9.19 us
    pallas_call x1, Pallas kernels, memory_mix(): pl.pallas_call(memory_kernel, grid=(seq // tb,), out_shape=jax.ShapeDtype...  7.54 us

profile of v1, /device:TPU:9, one launch (start us, length us, event | category | flops | bytes accessed | tf_op | source)
XLA Modules:
  0.0 176.3 jit_solution(17681842181061012544)
XLA Ops:
  0.0 0.8 copy.26
  0.8 1.2 copy-done.2
  2.0 0.9 copy-done.4
  3.0 0.9 copy-done.5
  3.9 0.9 copy-done.6
  4.8 0.9 copy-done.7
  5.7 0.9 copy-done.8
  6.6 0.9 copy-done.9
  7.5 0.9 copy-done.10
  8.4 78.3 %gather_all.1 = (bf16[1024,2048]{1,0:T(8,128)(2,1)S(1)}, f32[4,2,256]{2,1,0:T(2,128)S(1)}, bf16[2048,768]{1,0:T(8,128)(2,1)S(1)}, bf16[2048,384]{1,0:T(8,128)(2,1)S(1)}) custom-call(bf16[256,2048]{1,0:T(8,128)(2,1)S(1)} %bitcast.28, f32[4,2,256]{2,1,0:T(2,128)S(1)} %bitcast.29, bf16[128,512]{1,0:T(8,128)(2,1)S(1)} %copy-done.6, ...), custom_call_target="tpu_custom_call" | custom-call | tf_op jit(solution)/shard_map/gather_all/pallas_call | solution.py:506
  86.8 0.9 fusion
  87.7 3.5 %convolution_convert_fusion.q_ref.qk_ref.k_ref.v_ref.gate_ref = bf16[1024,768]{1,0:T(8,128)(2,1)S(1)} fusion(bf16[2048,768]{1,0:T(8,128)(2,1)S(1)} %get-tuple-element.10, bf16[1024,2048]{1,0:T(8,128)(2,1)S(1)} %get-tuple-element.9, f32[2048]{0:T(1024)S(1)} %copy-done.14, f32[1024]{0:T(1024)S(1)} %add_rsqrt_fusion), kind=kOutput, calls=%fused_computation.5 | convolution fusion | flops 3230400512 | bytes 8925184 | tf_op jit(solution)/shard_map/dot_general | solution.py:794
  91.2 1.1 slice_convert_fusion
  92.9 9.2 %subtract_convert_fusion.pool_ref = bf16[1024,256]{1,0:T(8,128)(2,1)S(1)} fusion(f32[1024,256]{1,0:T(8,128)} %slice_convert_fusion, s32[256]{0:T(256)S(1)} %get-tuple-element.43, s32[256]{0:T(256)S(1)} %get-tuple-element.44, f32[256]{0:T(256)S(1)} %get-tuple-element.27, f32[256]{0:T(256)S(1)} %get-tuple-element.28, f32[256]{0:T(256)S(1)} %get-tuple-element.29, ...), kind=kLoop, calls=%fused_computation.8 | loop fusion | flops 10747904 | bytes 1591296 | tf_op jit(solution)/shard_map/convert_element_type | solution.py:162
  102.3 3.4 %fusion.6 = f32[4,1024]{1,0:T(4,128)S(1)} fusion(bf16[1024,2048]{1,0:T(8,128)(2,1)} %copy-done.1, f32[2048]{0:T(1024)S(1)} %copy-done.14, f32[1024]{0:T(1024)S(1)} %add_rsqrt_fusion, bf16[4,1,2048]{2,1,0:T(2,128)(2,1)S(1)} %constant_dynamic-slice_fusion.3, f32[4]{0:T(128)S(1)} %dynamic-slice_reduce_fusion), kind=kOutput, calls=%fused_computation.7 | convolution fusion | flops 25169920 | bytes 4239376 | tf_op jit(solution)/shard_map/dot_general | solution.py:798
  105.8 1.2 reduce-window.48
  107.3 1.6 reduce-window.50
  111.0 1.0 copy.19.cols_ref
  112.7 1.2 constant_dynamic-slice_fusion.1
  113.9 1.3 constant_dynamic-slice_fusion.gain_ref
  115.2 7.5 %memory_mix.1.mem_ref = bf16[1024,128]{1,0:T(8,128)(2,1)} custom-call(bf16[1024,768]{1,0:T(8,128)(2,1)} %copy-done.11, bf16[1024,768]{1,0:T(8,128)(2,1)} %copy-done.11, bf16[1024,768]{1,0:T(8,128)(2,1)} %copy-done.11, bf16[1024,768]{1,0:T(8,128)(2,1)} %copy-done.11, bf16[1024,768]{1,0:T(8,128)(2,1)} %copy-done.11, f32[1024,5]{1,0:T(8,128)} %copy.19.cols_ref, ...), custom_call_target="tpu_custom_call" | custom-call | tf_op jit(solution)/shard_map/memory_mix/pallas_call | solution.py:617
  122.7 0.9 copy-done.3
  123.7 51.9 %project_out.1 = bf16[128,2048]{1,0:T(8,128)(2,1)S(1)} custom-call(bf16[1024,128]{1,0:T(8,128)(2,1)S(1)} %copy-done.3, bf16[1024,256]{1,0:T(8,128)(2,1)S(1)} %subtract_convert_fusion.pool_ref, bf16[2048,384]{1,0:T(8,128)(2,1)S(1)} %get-tuple-element.12.weight_ref), custom_call_target="tpu_custom_call" | custom-call | tf_op jit(solution)/shard_map/project_out/pallas_call | solution.py:729
  175.5 0.8 copy.28
  (57 shorter events, 3.7 us)
Async XLA Ops:
  0.0 112.0 %copy-start = (f32[1,2,4,128,128]{4,3,2,1,0:T(8,128)S(1)}, f32[1,2,4,128,128]{4,3,2,1,0:T(8,128)}, u32[]{:S(2)}) copy-start(f32[1,2,4,128,128]{4,3,2,1,0:T(8,128)} %param.24) | copy-start | bytes 1572868
  0.0 87.7 %copy-start.14 = (f32[2048]{0:T(1024)S(1)}, f32[2048]{0:T(1024)}, u32[]{:S(2)}) copy-start(f32[2048]{0:T(1024)} %param.16) | copy-start | bytes 24580
  0.8 1.2 copy-start.2
  2.0 0.9 copy-start.4
  3.0 0.9 copy-start.5
  3.9 0.9 copy-start.6
  4.8 0.9 copy-start.7
  5.7 0.9 copy-start.8
  6.6 0.9 copy-start.9
  7.5 0.9 copy-start.10
  86.8 4.4 %copy-start.1 = (bf16[1024,2048]{1,0:T(8,128)(2,1)}, bf16[1024,2048]{1,0:T(8,128)(2,1)S(1)}, u32[]{:S(2)}) copy-start(bf16[1024,2048]{1,0:T(8,128)(2,1)S(1)} %get-tuple-element.9) | copy-start | bytes 12582916
  87.7 14.4 %copy-start.12 = (bf16[4,4,2048]{2,1,0:T(4,128)(2,1)S(1)}, bf16[4,4,2048]{2,1,0:T(4,128)(2,1)}, u32[]{:S(2)}) copy-start(bf16[4,4,2048]{2,1,0:T(4,128)(2,1)} %param.21) | copy-start | bytes 196612
  87.7 14.4 %copy-start.13 = (f32[4,4]{1,0:T(4,128)S(1)}, f32[4,4]{1,0:T(4,128)}, u32[]{:S(2)}) copy-start(f32[4,4]{1,0:T(4,128)} %param.22) | copy-start | bytes 196
  91.2 1.5 copy-start.11
  122.7 0.9 copy-start.3

commit v2 on v1

--- a/solution.py
+++ b/solution.py
@@ -356,6 +356,8 @@
         swap_recv,
         row_send,
         row_recv,
+        relay_send,
+        relay_recv,
     ) = refs[6 + count :]
     sp, fs, tp = (lax.axis_index(name) for name in ("sp", "fs", "tp"))
     other = 1 - tp
@@ -364,16 +366,17 @@
     half = block // 2
     ups = [lax.rem(sp + k, n_sp) for k in range(n_sp)]
     downs = [lax.rem(sp + n_sp - k, n_sp) for k in range(n_sp)]
-    fs_up = [lax.rem(fs + j, n_fs) for j in range(n_fs)]
-    fs_down = [lax.rem(fs + n_fs - j, n_fs) for j in range(n_fs)]
+    beside = fs + 1 - 2 * lax.rem(fs, 2)
+    across = lax.rem(fs + 2, 4)
+    peers = (beside, across)
 
     barrier = pltpu.get_barrier_semaphore()
     for k in range(1, n_sp):
         pl.semaphore_signal(barrier, inc=1, device_id={"sp": ups[k]}, device_id_type=MESH)
-    for j in range(1, n_fs):
-        pl.semaphore_signal(barrier, inc=1, device_id={"fs": fs_up[j]}, device_id_type=MESH)
+    for peer in peers:
+        pl.semaphore_signal(barrier, inc=1, device_id={"fs": peer}, device_id_type=MESH)
     pl.semaphore_signal(barrier, inc=1, device_id={"tp": other}, device_id_type=MESH)
-    pl.semaphore_wait(barrier, n_sp + n_fs - 1)
+    pl.semaphore_wait(barrier, n_sp + 2)
 
     in_count = count - 2
     in_width = sum(widths[:in_count])
@@ -420,79 +423,132 @@
             device_id_type=MESH,
         )
 
-    def token_copy(k, target, source):
+    def token_copy(source, step):
+        at = aligned(source * block + tp * half, half)
         return pltpu.make_async_remote_copy(
-            src_ref=token_ref.at[aligned(tp * half, half)],
-            dst_ref=x_ref.at[aligned(source * block + tp * half, half)],
-            send_sem=token_send.at[k - 1],
-            recv_sem=token_recv.at[k - 1],
-            device_id={"sp": target},
+            src_ref=token_ref.at[aligned(tp * half, half)] if source is sp else x_ref.at[at],
+            dst_ref=x_ref.at[at],
+            send_sem=token_send.at[source * 2 + (step + 1) // 2],
+            recv_sem=token_recv.at[source],
+            device_id={"sp": sp + step},
             device_id_type=MESH,
         )
 
-    def swap_copy(k, side):
-        at = x_ref.at[aligned(downs[k] * block + side * half, half)]
+    def swap_copy(source, side):
+        at = x_ref.at[aligned(source * block + side * half, half)]
         return pltpu.make_async_remote_copy(
             src_ref=at,
             dst_ref=at,
-            send_sem=swap_send.at[k - 1],
-            recv_sem=swap_recv.at[k - 1],
+            send_sem=swap_send.at[source],
+            recv_sem=swap_recv.at[source],
             device_id={"tp": other},
             device_id_type=MESH,
         )
 
     def row_copies(k, j, at_fs):
         at = aligned((downs[k] * n_fs + at_fs) * rows, rows)
-        made = []
-        for which, ref in enumerate((in_ref, out_ref)):
-            made.append(
-                pltpu.make_async_remote_copy(
-                    src_ref=ref.at[at],
-                    dst_ref=ref.at[at],
-                    send_sem=row_send.at[k, j - 1, which],
-                    recv_sem=row_recv.at[k, j - 1, which],
-                    device_id={"fs": fs_up[j]},
-                    device_id_type=MESH,
-                )
+        return [
+            pltpu.make_async_remote_copy(
+                src_ref=ref.at[at],
+                dst_ref=ref.at[at],
+                send_sem=row_send.at[k, j, which],
+                recv_sem=row_recv.at[k, j, which],
+                device_id={"fs": peers[j]},
+                device_id_type=MESH,
             )
-        return made
+            for which, ref in enumerate((in_ref, out_ref))
+        ]
+
+    def relay_copies(k, j, at_fs):
+        part = rows // 2
+        at = aligned((downs[k] * n_fs + at_fs) * rows + j * part, part)
+        return [
+            pltpu.make_async_remote_copy(
+                src_ref=ref.at[at],
+                dst_ref=ref.at[at],
+                send_sem=relay_send.at[k, j, which],
+                recv_sem=relay_recv.at[k, j, which],
+                device_id={"fs": peers[j]},
+                device_id_type=MESH,
+            )
+            for which, ref in enumerate((in_ref, out_ref))
+        ]
+
+    def neighbour_sends(action):
+        for step in (1, -1):
+            @pl.when((sp + step >= 0) & (sp + step < n_sp))
+            def _(step=step):
+                action(token_copy(sp, step))
+
+    def arrivals(action, distances):
+        for distance in distances:
+            for step in (1, -1):
+                source = sp - step * distance
+                onward = sp + step
+
+                @pl.when((source >= 0) & (source < n_sp))
+                def _(source=source, onward=onward, step=step):
+                    action(source, onward, step)
+
+    def relay_tokens(source, onward, step):
+        token_copy(source, step).wait_recv()
+        swap_copy(source, tp).start()
+
+        @pl.when((onward >= 0) & (onward < n_sp))
+        def _():
+            token_copy(source, step).start()
+
+    def finish_tokens(source, onward, step):
+        swap_copy(source, other).wait_recv()
+        swap_copy(source, tp).wait_send()
+
+        @pl.when((onward >= 0) & (onward < n_sp))
+        def _():
+            token_copy(source, step).wait_send()
 
     for k in range(1, n_sp):
         for i in range(count):
             weight_copy(i, k, ups[k], sp).start()
     for k in range(1, n_sp):
         decay_copy(k, ups[k], sp).start()
-        token_copy(k, ups[k], sp).start()
+    neighbour_sends(lambda copy: copy.start())
     for copy in locals_:
         copy.wait()
     for k in range(n_sp):
         if k:
             for i in range(count):
                 weight_copy(i, k, ups[k], downs[k]).wait_recv()
-        for j in range(1, n_fs):
+        for j in range(2):
             for copy in row_copies(k, j, fs):
                 copy.start()
-    for k in range(1, n_sp):
-        token_copy(k, ups[k], downs[k]).wait_recv()
-        swap_copy(k, tp).start()
+    for k in range(n_sp):
+        for j in range(2):
+            for copy in row_copies(k, j, peers[j]):
+                copy.wait_recv()
+            for copy in relay_copies(k, 1 - j, peers[j]):
+                copy.start()
+        if k == n_sp - 2:
+            arrivals(relay_tokens, (1,))
+    arrivals(relay_tokens, range(2, n_sp))
     own_tokens.wait()
     own_decay.wait()
     for k in range(1, n_sp):
         decay_copy(k, ups[k], downs[k]).wait_recv()
-        swap_copy(k, other).wait_recv()
     for k in range(n_sp):
-        for j in range(1, n_fs):
-            for copy in row_copies(k, j, fs_down[j]):
+        for j in range(2):
+            for copy in relay_copies(k, j, 3 - fs):
                 copy.wait_recv()
+    arrivals(finish_tokens, range(1, n_sp))
+    neighbour_sends(lambda copy: copy.wait_send())
     for k in range(1, n_sp):
         for i in range(count):
             weight_copy(i, k, ups[k], sp).wait_send()
         decay_copy(k, ups[k], sp).wait_send()
-        token_copy(k, ups[k], sp).wait_send()
-        swap_copy(k, tp).wait_send()
     for k in range(n_sp):
-        for j in range(1, n_fs):
+        for j in range(2):
             for copy in row_copies(k, j, fs):
+                copy.wait_send()
+            for copy in relay_copies(k, j, peers[1 - j]):
                 copy.wait_send()
 
 
@@ -511,7 +567,7 @@
             jax.ShapeDtypeStruct((model_width, sum(widths[:-2])), tokens.dtype),
             jax.ShapeDtypeStruct((model_width, sum(widths[-2:])), tokens.dtype),
         ),
-        in_specs=[vmem] * (2 + count),
+        in_specs=[pl.BlockSpec(memory_space=pl.ANY)] * (2 + count),
         out_specs=(vmem,) * 4,
         scratch_shapes=[
             dma((count,)),
@@ -520,15 +576,17 @@
             dma((n_sp - 1, count)),
             dma((n_sp - 1,)),
             dma((n_sp - 1,)),
-            dma((n_sp - 1,)),
-            dma((n_sp - 1,)),
-            dma((n_sp - 1,)),
-            dma((n_sp - 1,)),
-            dma((n_sp, n_fs - 1, 2)),
-            dma((n_sp, n_fs - 1, 2)),
+            dma((2 * n_sp,)),
+            dma((n_sp,)),
+            dma((n_sp,)),
+            dma((n_sp,)),
+            dma((n_sp, 2, 2)),
+            dma((n_sp, 2, 2)),
+            dma((n_sp, 2, 2)),
+            dma((n_sp, 2, 2)),
         ],
         compiler_params=pltpu.CompilerParams(
-            collective_id=0, has_side_effects=True, vmem_limit_bytes=40 * 2**20
+            collective_id=0, has_side_effects=True, vmem_limit_bytes=60 * 2**20
         ),
         name="gather_all",
     )(tokens, decay, *weights)
@@ -637,7 +695,7 @@
 
 def project_kernel(
     n_sp, mem_ref, pool_ref, weight_ref, o_ref,
-    give, take, send, land, own, swap_send, swap_recv, z_send, z_recv,
+    give, take, send, land, total, own, swap_send, swap_recv, z_send, z_recv,
 ):
     sp, tp = lax.axis_index("sp"), lax.axis_index("tp")
     other = 1 - tp
@@ -670,52 +728,78 @@
             preferred_element_type=jnp.float32,
         )
 
-    def swap(k):
+    def swap(d):
         return pltpu.make_async_remote_copy(
-            src_ref=give.at[k],
-            dst_ref=take.at[k],
-            send_sem=swap_send.at[k],
-            recv_sem=swap_recv.at[k],
+            src_ref=give.at[d],
+            dst_ref=take.at[d],
+            send_sem=swap_send.at[d],
+            recv_sem=swap_recv.at[d],
             device_id={"tp": other},
             device_id_type=MESH,
         )
 
-    def pass_on(k):
+    low = 1 - (2 * sp) // n_sp
+    place = low * sp + (1 - low) * (n_sp - 1 - sp)
+
+    def pass_on(d, up):
+        slot = up * n_sp + d
         return pltpu.make_async_remote_copy(
-            src_ref=send.at[k - 1],
-            dst_ref=land.at[k - 1],
-            send_sem=z_send.at[k - 1],
-            recv_sem=z_recv.at[k - 1],
-            device_id={"sp": lax.rem(sp + k, n_sp)},
+            src_ref=send.at[d],
+            dst_ref=land.at[slot],
+            send_sem=z_send.at[d],
+            recv_sem=z_recv.at[slot],
+            device_id={"sp": sp + 2 * up - 1},
             device_id_type=MESH,
         )
 
-    order = list(range(1, n_sp)) + [0]
-    for k in order:
-        target = lax.rem(sp + k, n_sp)
-        for c in range(width // tile):
-            give[k, :, c * tile : (c + 1) * tile] = product(target, other, c).astype(jnp.bfloat16)
-        swap(k).start()
-    for k in order:
-        target = lax.rem(sp + k, n_sp)
-        swap(k).wait_recv()
-        for c in range(width // tile):
-            at = slice(c * tile, (c + 1) * tile)
-            both = product(target, tp, c) + take[k, :, at].astype(jnp.float32)
-            if k:
-                send[k - 1, :, at] = both.astype(jnp.bfloat16)
-            else:
-                own[:, at] = both
-        if k:
-            pass_on(k).start()
-    for k in range(1, n_sp):
-        pass_on(k).wait_recv()
-        own[...] += land[k - 1].astype(jnp.float32)
+    def actual(d):
+        return low * d + (1 - low) * (n_sp - 1 - d)
+
+    order = [(d, actual(d)) for d in range(n_sp - 1, -1, -1)]
+    tiles = [slice(c * tile, (c + 1) * tile) for c in range(width // tile)]
+    for _, target in order:
+        for c, at in enumerate(tiles):
+            give[target, :, at] = product(target, other, c).astype(jnp.bfloat16)
+        swap(target).start()
+    for d, target in order:
+        swap(target).wait_recv()
+        for c, at in enumerate(tiles):
+            total[:, at] = product(target, tp, c) + take[target, :, at].astype(jnp.float32)
+
+        @pl.when(place == d)
+        def _():
+            own[...] = total[...]
+
+        def forward(up, fed, target=target):
+            @pl.when(fed)
+            def _():
+                pass_on(target, up).wait_recv()
+                total[...] += land[up * n_sp + target].astype(jnp.float32)
+
+            send[target] = total[...].astype(jnp.bfloat16)
+            pass_on(target, up).start()
+
+        @pl.when(place < d)
+        def _():
+            forward(low, place > 0)
+
+        @pl.when(place > d)
+        def _():
+            forward(1 - low, place < n_sp - 1)
+
+    for up in (0, 1):
+        @pl.when(sp != (n_sp - 1) * (1 - up))
+        def _(up=up):
+            pass_on(sp, up).wait_recv()
+            own[...] += land[up * n_sp + sp].astype(jnp.float32)
+
     o_ref[...] = own[...].astype(jnp.bfloat16)
-    for k in range(n_sp):
-        swap(k).wait_send()
-        if k:
-            pass_on(k).wait_send()
+    for d, target in order:
+        swap(target).wait_send()
+
+        @pl.when(place != d)
+        def _(target=target):
+            pass_on(target, 0).wait_send()
 
 
 def project_out(memory_out, pool_out, weight):
@@ -725,7 +809,6 @@
     vmem = pl.BlockSpec(memory_space=pltpu.VMEM)
     dma = pltpu.SemaphoreType.DMA
     buffers = pltpu.VMEM((n_sp, half, width), jnp.bfloat16)
-    fewer = pltpu.VMEM((n_sp - 1, half, width), jnp.bfloat16)
     return pl.pallas_call(
         functools.partial(project_kernel, n_sp),
         out_shape=jax.ShapeDtypeStruct((half, width), jnp.bfloat16),
@@ -734,13 +817,14 @@
         scratch_shapes=[
             buffers,
             buffers,
-            fewer,
-            fewer,
+            buffers,
+            pltpu.VMEM((2 * n_sp, half, width), jnp.bfloat16),
+            pltpu.VMEM((half, width), jnp.float32),
             pltpu.VMEM((half, width), jnp.float32),
             dma((n_sp,)),
             dma((n_sp,)),
-            dma((n_sp - 1,)),
-            dma((n_sp - 1,)),
+            dma((n_sp,)),
+            dma((2 * n_sp,)),
         ],
         compiler_params=pltpu.CompilerParams(
             collective_id=1, has_side_effects=True, vmem_limit_bytes=40 * 2**20
@@ -852,7 +936,8 @@
             lax.axis_size("tp") == 2
             and heads == lax.axis_size("sp")
             and heads > 1
-            and lax.axis_size("fs") > 1
+            and lax.axis_size("fs") == 4
+            and heads % 2 == 0
             and width == 128
             and features % (128 * heads) == 0
             and args[0].shape[1] % 32 == 0

time: 177 us -> 154 us (0.87)
  the two profiles are of different devices: /device:TPU:9 before, /device:TPU:0 now
where the time goes in v2:
time: 154 us
  Pallas kernels  124 us (81%)
  other arithmetic  10.6 us (7%)
  local copies, waits for them, and re-layouts  9.52 us (6%)
  matrix products  8.84 us (6%)
    pallas_call x1, Pallas kernels, gather_all(): pl.pallas_call(functools.partial(gather_kernel, n_sp, n_fs, widths), out_...  72.3 us
    pallas_call x1, Pallas kernels, project_out(): pl.pallas_call(functools.partial(project_kernel, n_sp), out_shape=jax.Sha...  44.4 us
    pallas_call x1, Pallas kernels, memory_mix(): pl.pallas_call(memory_kernel, grid=(seq // tb,), out_shape=jax.ShapeDtype...  7.64 us
    dot_general x1, matrix products, by_head(): jnp.dot(normed, in_weight, preferred_element_type=jnp.float32)  5.39 us
    unnamed x20, local copies, waits for them, and re-layouts  4.49 us
    another operation x8, other arithmetic  3.51 us
    dot_general x1, matrix products, by_head(): lax.dot_general(own_gates, normed, (((1,), (1,)), ((), ())), preferred_el...  3.45 us
    reduce_sum x1, other arithmetic, by_head(): jnp.mean(flattened * flattened, axis=-1, keepdims=True) + norm_eps  3.22 us

profile of v2, /device:TPU:0, one launch (start us, length us, event | category | flops | bytes accessed | tf_op | source)
XLA Modules:
  0.0 153.6 jit_solution(1939085400785831542)
XLA Ops:
  0.0 1.4 copy.26
  1.4 72.3 %gather_all.1 = (bf16[1024,2048]{1,0:T(8,128)(2,1)}, f32[4,2,256]{2,1,0:T(2,128)}, bf16[2048,768]{1,0:T(8,128)(2,1)}, bf16[2048,384]{1,0:T(8,128)(2,1)}) custom-call(bf16[256,2048]{1,0:T(8,128)(2,1)} %bitcast.28, f32[4,2,256]{2,1,0:T(2,128)} %bitcast.37, bf16[128,512]{1,0:T(8,128)(2,1)} %refs_2_.1, bf16[128,512]{1,0:T(8,128)(2,1)} %refs_3_.1, ...), custom_call_target="tpu_custom_call" | custom-call | tf_op jit(solution)/shard_map/gather_all/pallas_call | solution.py:562
  73.7 3.2 %fusion = f32[1024]{0:T(1024)S(1)} fusion(bf16[1024,2048]{1,0:T(8,128)(2,1)} %get-tuple-element.9), kind=kLoop, calls=%fused_computation.2 | loop fusion | flops 6290432 | bytes 4198400 | tf_op jit(solution)/shard_map/reduce_sum | solution.py:875
  76.9 0.2 copy-done.4
  77.1 5.4 %convolution_convert_fusion.q_ref.qk_ref.k_ref.v_ref.gate_ref = bf16[1024,768]{1,0:T(8,128)(2,1)S(1)} fusion(bf16[2048,768]{1,0:T(8,128)(2,1)} %get-tuple-element.10, bf16[1024,2048]{1,0:T(8,128)(2,1)S(1)} %copy-done.4, f32[2048]{0:T(1024)S(1)} %copy-done.8, f32[1024]{0:T(1024)S(1)} %add_rsqrt_fusion), kind=kOutput, calls=%fused_computation.5 | convolution fusion | flops 3230400512 | bytes 8925184 | tf_op jit(solution)/shard_map/dot_general | solution.py:878
  82.5 1.2 copy-done.3
  84.0 2.7 %subtract_convert_fusion.pool_ref = bf16[1024,256]{1,0:T(8,128)(2,1)S(1)} fusion(f32[1024,256]{1,0:T(8,128)S(1)} %slice_convert_fusion, s32[256]{0:T(256)S(1)} %get-tuple-element.43, s32[256]{0:T(256)S(1)} %get-tuple-element.44, f32[256]{0:T(256)S(1)} %get-tuple-element.27, f32[256]{0:T(256)S(1)} %get-tuple-element.28, f32[256]{0:T(256)S(1)} %get-tuple-element.29, ...), kind=kLoop, calls=%fused_computation.8 | loop fusion | flops 10747904 | bytes 1591296 | tf_op jit(solution)/shard_map/convert_element_type | solution.py:162
  86.8 0.2 dynamic-slice_reduce_fusion
  87.0 3.5 %fusion.6 = f32[4,1024]{1,0:T(4,128)S(1)} fusion(bf16[1024,2048]{1,0:T(8,128)(2,1)} %get-tuple-element.9, f32[2048]{0:T(1024)S(1)} %copy-done.8, f32[1024]{0:T(1024)S(1)} %add_rsqrt_fusion, bf16[4,1,2048]{2,1,0:T(2,128)(2,1)S(1)} %constant_dynamic-slice_fusion.3, f32[4]{0:T(128)S(1)} %dynamic-slice_reduce_fusion), kind=kOutput, calls=%fused_computation.7 | convolution fusion | flops 25169920 | bytes 4239376 | tf_op jit(solution)/shard_map/dot_general | solution.py:882
  90.5 1.2 reduce-window.48
  92.0 1.6 %reduce-window.50 = f32[8,128]{1,0:T(8,128)S(1)} reduce-window(f32[8,128]{1,0:T(8,128)S(1)} %get-tuple-element.13, f32[]{:T(128)} %constant.43.clone.1), window={size=1x128 pad=0_0x0_127}, to_apply=%region_7.8 | reduce-window | flops 130048 | bytes 8196 | tf_op jit(solution)/shard_map/reduce-window.6
  93.8 0.3 reduce-window.34
  94.2 0.1 slice_reduce_fusion.3
  94.4 0.3 reduce-window.36
  94.8 0.1 slice_reduce_fusion.2
  95.0 0.6 pad_maximum_fusion.rows_ref
  95.6 1.0 copy.19.cols_ref
  96.7 0.7 constant_dynamic-slice_fusion.2
  97.3 1.3 constant_dynamic-slice_fusion.1
  98.6 1.2 constant_dynamic-slice_fusion.gain_ref
  99.8 7.6 %memory_mix.1.mem_ref = bf16[1024,128]{1,0:T(8,128)(2,1)} custom-call(bf16[1024,768]{1,0:T(8,128)(2,1)} %copy-done.3, bf16[1024,768]{1,0:T(8,128)(2,1)} %copy-done.3, bf16[1024,768]{1,0:T(8,128)(2,1)} %copy-done.3, bf16[1024,768]{1,0:T(8,128)(2,1)} %copy-done.3, bf16[1024,768]{1,0:T(8,128)(2,1)} %copy-done.3, f32[1024,5]{1,0:T(8,128)} %copy.19.cols_ref, ...), custom_call_target="tpu_custom_call" | custom-call | tf_op jit(solution)/shard_map/memory_mix/pallas_call | solution.py:675
  107.4 0.9 copy-done.2
  108.4 44.4 %project_out.1 = bf16[128,2048]{1,0:T(8,128)(2,1)S(1)} custom-call(bf16[1024,128]{1,0:T(8,128)(2,1)S(1)} %copy-done.2, bf16[1024,256]{1,0:T(8,128)(2,1)S(1)} %subtract_convert_fusion.pool_ref, bf16[2048,384]{1,0:T(8,128)(2,1)S(1)} %copy-done.1), custom_call_target="tpu_custom_call" | custom-call | tf_op jit(solution)/shard_map/project_out/pallas_call | solution.py:812
  152.8 0.8 copy.28
  (45 shorter events, 1.2 us)
Async XLA Ops:
  0.0 96.7 %copy-start = (f32[1,2,4,128,128]{4,3,2,1,0:T(8,128)S(1)}, f32[1,2,4,128,128]{4,3,2,1,0:T(8,128)}, u32[]{:S(2)}) copy-start(f32[1,2,4,128,128]{4,3,2,1,0:T(8,128)} %param.24) | copy-start | bytes 1572868
  0.0 76.9 %copy-start.8 = (f32[2048]{0:T(1024)S(1)}, f32[2048]{0:T(1024)}, u32[]{:S(2)}) copy-start(f32[2048]{0:T(1024)} %param.16) | copy-start | bytes 24580
  73.7 3.5 %copy-start.4 = (bf16[1024,2048]{1,0:T(8,128)(2,1)S(1)}, bf16[1024,2048]{1,0:T(8,128)(2,1)}, u32[]{:S(2)}) copy-start(bf16[1024,2048]{1,0:T(8,128)(2,1)} %get-tuple-element.9) | copy-start | bytes 12582916
  77.1 9.6 %copy-start.5 = (bf16[4,4,2048]{2,1,0:T(4,128)(2,1)S(1)}, bf16[4,4,2048]{2,1,0:T(4,128)(2,1)}, u32[]{:S(2)}) copy-start(bf16[4,4,2048]{2,1,0:T(4,128)(2,1)} %param.21) | copy-start | bytes 196612
  77.1 9.6 %copy-start.7 = (f32[4,4]{1,0:T(4,128)S(1)}, f32[4,4]{1,0:T(4,128)}, u32[]{:S(2)}) copy-start(f32[4,4]{1,0:T(4,128)} %param.22) | copy-start | bytes 196
  82.5 1.2 copy-start.3
  86.7 3.8 %copy-start.6 = (f32[4,2,256]{2,1,0:T(2,128)S(1)}, f32[4,2,256]{2,1,0:T(2,128)}, u32[]{:S(2)}) copy-start(f32[4,2,256]{2,1,0:T(2,128)} %get-tuple-element.11) | copy-start | bytes 24580
  99.8 7.6 %copy-start.1 = (bf16[2048,384]{1,0:T(8,128)(2,1)S(1)}, bf16[2048,384]{1,0:T(8,128)(2,1)}, u32[]{:S(2)}) copy-start(bf16[2048,384]{1,0:T(8,128)(2,1)} %get-tuple-element.12.weight_ref) | copy-start | bytes 4718596
  107.4 1.0 copy-start.2

commit v3 on v2

--- a/solution.py
+++ b/solution.py
@@ -592,15 +592,98 @@
     )(tokens, decay, *weights)
 
 
+def input_kernel(x_ref, gain_ref, weight_ref, gates_ref, bias_ref, proj_ref, pre_ref):
+    wide = x_ref[...].astype(jnp.float32)
+    normed = (
+        wide
+        * lax.rsqrt(jnp.mean(wide * wide, axis=-1, keepdims=True) + norm_eps)
+        * gain_ref[...]
+    ).astype(jnp.bfloat16)
+    proj_ref[...] = jnp.dot(
+        normed, weight_ref[...], preferred_element_type=jnp.float32
+    ).astype(jnp.bfloat16)
+    pre_ref[...] = (
+        lax.dot_general(
+            normed, gates_ref[...], (((1,), (1,)), ((), ())), preferred_element_type=jnp.float32
+        )
+        + bias_ref[...]
+    )
+
+
+def project_in(x, norm_gain, weight, gates, bias):
+    seq, width = x.shape
+    tb = math.gcd(seq, 256)
+
+    def fixed(array):
+        return pl.BlockSpec(array.shape, lambda t: (0, 0))
+
+    def rows(columns):
+        return pl.BlockSpec((tb, columns), lambda t: (t, 0))
+
+    norm_gain = norm_gain[None]
+    return pl.pallas_call(
+        input_kernel,
+        grid=(seq // tb,),
+        out_shape=(
+            jax.ShapeDtypeStruct((seq, weight.shape[1]), jnp.bfloat16),
+            jax.ShapeDtypeStruct((seq, gates.shape[0]), jnp.float32),
+        ),
+        in_specs=[rows(width), fixed(norm_gain), fixed(weight), fixed(gates), fixed(bias)],
+        out_specs=(rows(weight.shape[1]), rows(gates.shape[0])),
+        name="project_in",
+    )(x, norm_gain, weight, gates, bias)
+
+
+def scan_lanes(x, combine_, fill, reverse):
+    length = x.shape[1]
+    lane = lax.broadcasted_iota(jnp.int32, x.shape, 1)
+    d = 1
+    while d < length:
+        if reverse:
+            moved = jnp.where(lane < length - d, pltpu.roll(x, length - d, 1), fill)
+        else:
+            moved = jnp.where(lane >= d, pltpu.roll(x, d, 1), fill)
+        x = combine_(x, moved)
+        d *= 2
+    return x
+
+
+def prepare_gates(pre_ref, decay_ref, cols_ref, rows_ref, flat_ref):
+    gates = pre_ref[...].T[:8]
+    forget = jnp.minimum(gates, 0.0) - jnp.log1p(jnp.exp(-jnp.abs(gates))) + decay_ref[...]
+    front_sum = scan_lanes(forget, jnp.add, 0.0, False)[1:2]
+    rear_sum = scan_lanes(forget, jnp.add, 0.0, True)[3:4]
+    front_level = gates - front_sum
+    rear_level = gates - rear_sum
+    front_peak = scan_lanes(front_level, jnp.maximum, 0.0, False)[0:1]
+    rear_peak = scan_lanes(rear_level, jnp.maximum, 0.0, True)[2:3]
+    front_peak = jnp.maximum(front_peak, 0.0)
+    rear_peak = jnp.maximum(rear_peak, 0.0)
+    rows_ref[0:1, :] = front_level[0:1]
+    rows_ref[1:2, :] = rear_level[2:3]
+    flat_ref[...] = jnp.zeros_like(flat_ref)
+    flat_ref[0:1, :] = front_peak
+    flat_ref[1:2, :] = rear_peak
+    flat_ref[2:3, :] = front_sum + front_peak
+    flat_ref[3:4, :] = rear_sum + rear_peak
+    flat_ref[4:5, :] = rear_level[2:3]
+    cols_ref[...] = flat_ref[...].T
+
+
 def memory_kernel(
-    q_ref, qk_ref, k_ref, v_ref, gate_ref, cols_ref, rows_ref, mem_ref, norm_ref, gain_ref, o_ref
+    q_ref, qk_ref, k_ref, v_ref, gate_ref, pre_ref, decay_ref, mem_ref, norm_ref, gain_ref, o_ref,
+    cols_ref, rows_ref, flat_ref,
 ):
+    @pl.when(pl.program_id(0) == 0)
+    def _():
+        prepare_gates(pre_ref, decay_ref, cols_ref, rows_ref, flat_ref)
+
     tb = q_ref.shape[0]
     seq = k_ref.shape[0]
     width = q_ref.shape[1]
     scale = width ** (-0.5)
     q = q_ref[...]
-    cols = cols_ref[...]
+    cols = cols_ref[pl.ds(pl.multiple_of(pl.program_id(0) * tb, tb), tb), :]
     front_peak, rear_peak = cols[:, 0:1], cols[:, 1:2]
     front_max, rear_max = cols[:, 2:3], cols[:, 3:4]
     rear_own = cols[:, 4:5]
@@ -660,7 +743,7 @@
     o_ref[...] = (normed * jax.nn.sigmoid(gate_ref[...].astype(jnp.float32))).astype(jnp.bfloat16)
 
 
-def memory_mix(proj, cols, rows, memory, normalizer, gain, width):
+def memory_mix(proj, pre, decay, memory, normalizer, gain, width):
     seq = proj.shape[0]
     tb = math.gcd(seq, 256)
 
@@ -682,15 +765,20 @@
             part(1, True),
             part(2, True),
             part(3, False),
-            pl.BlockSpec((tb, cols.shape[1]), lambda t: (t, 0)),
-            fixed(rows),
+            fixed(pre),
+            fixed(decay),
             fixed(memory),
             fixed(normalizer),
             fixed(gain),
         ],
         out_specs=pl.BlockSpec((tb, width), lambda t: (t, 0)),
+        scratch_shapes=[
+            pltpu.VMEM((seq, 128), jnp.float32),
+            pltpu.VMEM((8, seq), jnp.float32),
+            pltpu.VMEM((128, seq), jnp.float32),
+        ],
         name="memory_mix",
-    )(proj, proj, proj, proj, proj, cols, rows, memory, normalizer, gain)
+    )(proj, proj, proj, proj, proj, pre, decay, memory, normalizer, gain)
 
 
 def project_kernel(
@@ -854,6 +942,10 @@
     width = head_gain.shape[1]
     n_sp = lax.axis_size("sp")
     sp, tp = lax.axis_index("sp"), lax.axis_index("tp")
+    own_gates = lax.dynamic_index_in_dim(gate_weight, sp, 1, keepdims=False)
+    own_gates = jnp.pad(own_gates, ((0, 124), (0, 0)))
+    own_bias = lax.dynamic_index_in_dim(gate_bias, sp, 1, keepdims=False)
+    own_bias = jnp.pad(own_bias, (0, 124))[None]
     everything, decay, in_weight, out_weight = gather_all(
         tokens[0],
         decay_extra[0].transpose(1, 0, 2),
@@ -868,37 +960,15 @@
         ),
     )
     seq = everything.shape[0]
-    decay = decay.transpose(1, 0, 2).reshape(2, seq)
-    flattened = everything.astype(jnp.float32)
-    normed = (
-        flattened
-        * lax.rsqrt(jnp.mean(flattened * flattened, axis=-1, keepdims=True) + norm_eps)
-        * norm_gain
-    ).astype(jnp.bfloat16)
-    proj = jnp.dot(normed, in_weight, preferred_element_type=jnp.float32).astype(jnp.bfloat16)
-    own_gates = lax.dynamic_index_in_dim(gate_weight, sp, 1, keepdims=False)
-    own_bias = lax.dynamic_index_in_dim(gate_bias, sp, 1, keepdims=True)
-    gate_pre = (
-        lax.dot_general(
-            own_gates, normed, (((1,), (1,)), ((), ())), preferred_element_type=jnp.float32
-        )
-        + own_bias
-    )
-    front_sum = lax.cumsum(jax.nn.log_sigmoid(gate_pre[1]) + decay[0])
-    rear_sum = lax.cumsum(jax.nn.log_sigmoid(gate_pre[3]) + decay[1], reverse=True)
-    front_level = gate_pre[0] - front_sum
-    rear_level = gate_pre[2] - rear_sum
-    front_peak = jnp.maximum(lax.cummax(front_level), 0.0)
-    rear_peak = jnp.maximum(lax.cummax(rear_level, reverse=True), 0.0)
-    rows = jnp.stack([front_level, rear_level])
-    cols = jnp.stack(
-        [front_peak, rear_peak, front_sum + front_peak, rear_sum + rear_peak, rear_level]
-    ).T
+    decay = decay.transpose(1, 0, 2).reshape(2, 1, seq)
+    decay = jnp.pad(decay, ((0, 0), (1, 0), (0, 0))).reshape(4, seq)
+    decay = jnp.pad(decay, ((0, 4), (0, 0)))
+    proj, pre = project_in(everything, norm_gain, in_weight, own_gates, own_bias)
     memory = lax.dynamic_index_in_dim(init_memory[0], sp, 1, keepdims=False)
     normalizer = lax.dynamic_index_in_dim(init_normalizer[0], sp, 1, keepdims=False)
     gain = lax.dynamic_slice_in_dim(head_gain, sp, 1, 0)
     memory_out = memory_mix(
-        proj, cols, rows, memory.reshape(2 * width, width), normalizer, gain, width
+        proj, pre, decay, memory.reshape(2 * width, width), normalizer, gain, width
     )
     pool_input = proj[:, 4 * width :]
     features = pool_input.shape[1]

time: 154 us -> 149 us (0.968)
  Pallas kernels: 124 us -> 135 us
  matrix products: 8.84 us -> 0 us
  other arithmetic: 10.6 us -> 3.79 us
    pallas_call x0 -> x1, Pallas kernels: none -> 9.17 us  [project_in(): pl.pallas_call(input_kernel, grid=(seq // tb,), out_shape=(jax.ShapeDtype...]
    dot_general x2 -> x0, matrix products: 8.84 us -> none  [the longest x1 5.39 us: by_head(): jnp.dot(normed, in_weight, preferred_element_type=jnp.float32)]
    another operation x9 -> x0, other arithmetic: 4.12 us -> none
    reduce_sum x1 -> x0, other arithmetic: 3.22 us -> none  [by_head(): jnp.mean(flattened * flattened, axis=-1, keepdims=True) + norm_eps]
    unnamed x20 -> x12, local copies, waits for them, and re-layouts: 4.49 us -> 3.07 us
where the time goes in v3:
time: 149 us
  Pallas kernels  135 us (91%)
  local copies, waits for them, and re-layouts  10.1 us (7%)
  other arithmetic  3.79 us (3%)
    pallas_call x1, Pallas kernels, gather_all(): pl.pallas_call(functools.partial(gather_kernel, n_sp, n_fs, widths), out_...  72.3 us
    pallas_call x1, Pallas kernels, project_out(): pl.pallas_call(functools.partial(project_kernel, n_sp), out_shape=jax.Sha...  44.3 us
    pallas_call x1, Pallas kernels, project_in(): pl.pallas_call(input_kernel, grid=(seq // tb,), out_shape=(jax.ShapeDtype...  9.17 us
    pallas_call x1, Pallas kernels, memory_mix(): pl.pallas_call(memory_kernel, grid=(seq // tb,), out_shape=jax.ShapeDtype...  9.11 us
    unnamed x12, local copies, waits for them, and re-layouts  3.07 us

profile of v3, /device:TPU:0, one launch (start us, length us, event | category | flops | bytes accessed | tf_op | source)
XLA Modules:
  0.0 148.9 jit_solution(16439596497794252155)
XLA Ops:
  0.0 0.0 copy-start
  0.0 0.9 constant_dynamic-slice_fusion.3
  1.0 0.8 pad.20.gates_ref
  1.8 0.9 dynamic-slice_reduce_fusion
  2.7 0.6 pad_bitcast_fusion.bias_ref
  3.2 1.3 copy.24
  4.5 72.3 %gather_all.1 = (bf16[1024,2048]{1,0:T(8,128)(2,1)}, f32[4,2,256]{2,1,0:T(2,128)}, bf16[2048,768]{1,0:T(8,128)(2,1)}, bf16[2048,384]{1,0:T(8,128)(2,1)}) custom-call(bf16[256,2048]{1,0:T(8,128)(2,1)} %bitcast.19, f32[4,2,256]{2,1,0:T(2,128)} %bitcast.22, bf16[128,512]{1,0:T(8,128)(2,1)} %refs_2_.1, bf16[128,512]{1,0:T(8,128)(2,1)} %refs_3_.1, ...), custom_call_target="tpu_custom_call" | custom-call | tf_op jit(solution)/shard_map/gather_all/pallas_call | solution.py:562
  76.8 9.2 %project_in.1 = (bf16[1024,768]{1,0:T(8,128)(2,1)}, f32[1024,128]{1,0:T(8,128)}) custom-call(bf16[1024,2048]{1,0:T(8,128)(2,1)} %get-tuple-element.11.x_ref, f32[1,2048]{1,0:T(1,128)} %bitcast.23, bf16[2048,768]{1,0:T(8,128)(2,1)} %get-tuple-element.12.weight_ref, bf16[128,2048]{1,0:T(8,128)(2,1)} %pad.20.gates_ref, f32[1,128]{1,0:T(1,128)} %pad_bitcast_fusion.bias_ref), custom_call_target="tpu_custom_call" | custom-call | tf_op jit(solution)/shard_map/project_in/pallas_call | solution.py:624
  86.0 0.0 copy-start.3
  86.0 1.1 slice_convert_fusion
  87.3 2.5 %subtract_convert_fusion.pool_ref = bf16[1024,256]{1,0:T(8,128)(2,1)S(1)} fusion(f32[1024,256]{1,0:T(8,128)S(1)} %slice_convert_fusion, s32[256]{0:T(256)S(1)} %get-tuple-element.33, s32[256]{0:T(256)S(1)} %get-tuple-element.34, f32[256]{0:T(256)S(1)} %get-tuple-element.17, f32[256]{0:T(256)S(1)} %get-tuple-element.18, f32[256]{0:T(256)S(1)} %get-tuple-element.19, ...), kind=kLoop, calls=%fused_computation | loop fusion | flops 10747904 | bytes 1591296 | tf_op jit(solution)/shard_map/convert_element_type | solution.py:162
  89.9 0.0 copy-done
  89.9 0.7 constant_dynamic-slice_fusion.2
  90.6 1.2 constant_dynamic-slice_fusion.1
  91.8 1.3 constant_dynamic-slice_fusion.gain_ref
  93.0 0.0 copy-done.3
  93.1 0.6 pad.23.decay_ref
  93.7 0.0 copy-start.1
  93.7 9.1 %memory_mix.1.mem_ref = bf16[1024,128]{1,0:T(8,128)(2,1)} custom-call(bf16[1024,768]{1,0:T(8,128)(2,1)} %get-tuple-element.13.q_ref.qk_ref.k_ref.v_ref.gate_ref, bf16[1024,768]{1,0:T(8,128)(2,1)} %get-tuple-element.13.q_ref.qk_ref.k_ref.v_ref.gate_ref, bf16[1024,768]{1,0:T(8,128)(2,1)} %get-tuple-element.13.q_ref.qk_ref.k_ref.v_ref.gate_ref, ...), custom_call_target="tpu_custom_call" | custom-call | tf_op jit(solution)/shard_map/memory_mix/pallas_call | solution.py:758
  102.8 0.0 copy-done.1
  102.8 0.0 copy-start.2
  102.9 0.9 copy-done.2
  103.8 44.3 %project_out.1 = bf16[128,2048]{1,0:T(8,128)(2,1)S(1)} custom-call(bf16[1024,128]{1,0:T(8,128)(2,1)S(1)} %copy-done.2, bf16[1024,256]{1,0:T(8,128)(2,1)S(1)} %subtract_convert_fusion.pool_ref, bf16[2048,384]{1,0:T(8,128)(2,1)S(1)} %copy-done.1), custom_call_target="tpu_custom_call" | custom-call | tf_op jit(solution)/shard_map/project_out/pallas_call | solution.py:900
  148.2 0.8 copy.26
  (13 shorter events, 0.2 us)
Async XLA Ops:
  0.0 89.9 %copy-start = (f32[1,2,4,128,128]{4,3,2,1,0:T(8,128)S(1)}, f32[1,2,4,128,128]{4,3,2,1,0:T(8,128)}, u32[]{:S(2)}) copy-start(f32[1,2,4,128,128]{4,3,2,1,0:T(8,128)} %param.24) | copy-start | bytes 1572868
  86.0 7.0 %copy-start.3 = (f32[4,2,256]{2,1,0:T(2,128)S(1)}, f32[4,2,256]{2,1,0:T(2,128)}, u32[]{:S(2)}) copy-start(f32[4,2,256]{2,1,0:T(2,128)} %get-tuple-element.15) | copy-start | bytes 24580
  93.7 9.1 %copy-start.1 = (bf16[2048,384]{1,0:T(8,128)(2,1)S(1)}, bf16[2048,384]{1,0:T(8,128)(2,1)}, u32[]{:S(2)}) copy-start(bf16[2048,384]{1,0:T(8,128)(2,1)} %get-tuple-element.16.weight_ref) | copy-start | bytes 4718596
  102.8 1.0 copy-start.2
